TPU v7x, 512 devices: a whole 4x4x16 slice. The times are simulated.
512 devices in a mesh: kv: 64 (over z, y), tp: 8 (over x, core).
Axes of the slice: x: 4, y: 4, z: 16, core: 2. Of those that a mesh axis runs over, the one named last changes fastest.
Arguments:
- tokens: bfloat16 [256, 4096], P(None, 'kv')
- lengths: int32 [64], replicated, may hold values from 1 to 4, 112 in all
- memory: float32 [64, 16, 128, 128], P('kv', 'tp'), may hold values from -0.6 to 0.6
- norm_gain: float32 [4096], P('kv'), may hold values from 0.1 to 1.9
- w_query: bfloat16 [4096, 2048], P('kv', 'tp'), may hold values from -0.09375 to 0.09375
- w_key: bfloat16 [4096, 2048], P('kv', 'tp'), may hold values from -0.09375 to 0.09375
- w_value: bfloat16 [4096, 2048], P('kv', 'tp'), may hold values from -0.09375 to 0.09375
- w_outgate: bfloat16 [4096, 2048], P('kv', 'tp'), may hold values from -0.09375 to 0.09375
- w_alpha: bfloat16 [4096, 16], P('kv'), may hold values from -0.09375 to 0.09375
- w_beta: bfloat16 [4096, 16], P('kv'), may hold values from -0.09375 to 0.09375
- decay_log: float32 [16], P('tp'), may hold values from -4 to 0.5
- decay_bias: float32 [16], P('tp'), may hold values from -1 to 1
- head_gain: float32 [128], replicated, may hold values from 0.1 to 1.9
- w_output: bfloat16 [2048, 4096], P('tp', 'kv'), may hold values from -0.125 to 0.125
- mlp_gain: float32 [4096], P('kv'), may hold values from 0.1 to 1.9
- w_gate: bfloat16 [4096, 11264], P('kv', 'tp'), may hold values from -0.09375 to 0.09375
- w_up: bfloat16 [4096, 11264], P('kv', 'tp'), may hold values from -0.09375 to 0.09375
- w_down: bfloat16 [11264, 4096], P('tp', 'kv'), may hold values from -0.0546875 to 0.0546875
Outputs:
- layer_out: bfloat16 [256, 4096], P(None, 'kv')
- new_memory: float32 [64, 16, 128, 128], P('kv', 'tp')
Inputs may be any that keep to these rules, and one draw needn't show every extreme that they name: How many of a sequence's 4 slots hold live tokens; the live ones come first; the lengths add up to seven quarters of 64, rounded down.
All inputs are finite; a program needn't handle non-finite values.
Results may differ from a plain program's by a relative error of at most 0.012.
Values may be sent and summed in bfloat16 or wider, within the bound.
A program may use at most 64 MiB of HBM per device.

v0:
```python
import math

import jax
import jax.numpy as jnp
from jax import lax
from jax.sharding import Mesh
from jax.sharding import PartitionSpec as P

D = 4096
DK = 128
DV = 128
NEW = 4
KV = ("kv_0", "kv_1")


epsilon = 1e-06


def split_up(shard, dim, peers):
    before, after = (shard.shape[:dim], shard.shape[dim + 1 :])
    return jnp.moveaxis(shard.reshape(*before, peers, -1, *after), dim, 0)


def sent_and_summed(shard, axis, dim):
    parts = split_up(shard, dim, lax.axis_size(axis))
    arrived = lax.all_to_all(parts, axis, split_axis=0, concat_axis=0, tiled=True)
    return arrived.astype(jnp.float32).sum(axis=0)


def in_one_piece(arrays, axis, dim, along):
    widths = [math.prod(a.shape[along:]) for a in arrays]
    both = jnp.concatenate(
        [a.reshape(*a.shape[:along], w) for a, w in zip(arrays, widths)], axis=along
    )
    filled = sent_and_summed(both, axis, dim)
    parts = jnp.split(filled, [sum(widths[:k]) for k in range(1, len(widths))], axis=along)
    return tuple(
        (b.reshape(*filled.shape[:along], *a.shape[along:]) for a, b in zip(arrays, parts))
    )


def copy_for_each(shard, axis):
    peers = lax.axis_size(axis)
    return lax.all_to_all(
        jnp.broadcast_to(shard[None], (peers, *shard.shape)), axis, 0, 0, tiled=True
    )


def joined_along(parts, dim):
    parts = jnp.moveaxis(parts, 0, dim)
    dims = parts.shape
    return parts.reshape(*dims[:dim], dims[dim] * dims[dim + 1], *dims[dim + 2 :])


def collect(shard, axis, dim):
    parts = copy_for_each(shard, axis)
    return joined_along(parts, dim)


def of_everyone(shard, axis):
    return copy_for_each(shard, axis).sum(axis=0)


def gather_in_order(shard, axes, order):
    parts = shard[None]
    for k in order:
        parts = lax.all_gather(parts, axes[k], axis=0, tiled=True)
    carried = [lax.axis_size(axes[k]) for k in reversed(order)]
    parts = parts.reshape(*carried, *shard.shape)
    turned = sorted(range(len(order)), key=lambda place: order[len(order) - 1 - place])
    return parts.transpose(*turned, *range(len(order), parts.ndim)).reshape(-1, *shard.shape)


def gather_axes(shard, axes, order, dim):
    return joined_along(gather_in_order(shard, axes, order), dim)


def over_copies(shard, axis):
    everything = copy_for_each(shard, axis)
    return jnp.sum(everything.astype(jnp.float32), axis=0)


def unit_rows(values):
    return values * lax.rsqrt(jnp.sum(values * values, axis=-1, keepdims=True) + epsilon)


def advance(memory, queries, key_rows, value_rows, decays, betas):
    outputs = []
    for step in range(queries.shape[1]):
        memory = jnp.exp(decays[:, step])[:, :, None, None] * memory
        predicted = jnp.einsum(
            "shde,shd->she", memory, key_rows[:, step], precision=lax.Precision.HIGHEST
        )
        correction = betas[:, step][:, :, None] * (value_rows[:, step] - predicted)
        memory = memory + key_rows[:, step][:, :, :, None] * correction[:, :, None, :]
        outputs.append(
            jnp.einsum("shde,shd->she", memory, queries[:, step], precision=lax.Precision.HIGHEST)
        )
    return (memory, jnp.stack(outputs, axis=1))


def per_device(
    tokens,
    lengths,
    memory,
    norm_gain,
    w_query,
    w_key,
    w_value,
    w_outgate,
    w_alpha,
    w_beta,
    decay_log,
    decay_bias,
    head_gain,
    w_output,
    mlp_gain,
    w_gate,
    w_up,
    w_down,
):
    total_rows = tokens.shape[0]
    kv_count = lax.axis_size(KV)
    kv_place = lax.axis_index(KV)
    tp_place = lax.axis_index("tp")
    own_rows = total_rows // kv_count
    seq_dev = memory.shape[0]
    heads_dev = memory.shape[1]
    token_f = tokens.astype(jnp.float32)
    squares = jnp.sum(token_f * token_f, axis=1)
    scaled = (token_f * norm_gain).astype(jnp.bfloat16)
    part_query = jnp.dot(scaled, w_query, preferred_element_type=jnp.float32)
    part_key = jnp.dot(scaled, w_key, preferred_element_type=jnp.float32)
    part_value = jnp.dot(scaled, w_value, preferred_element_type=jnp.float32)
    part_gate = jnp.dot(scaled, w_outgate, preferred_element_type=jnp.float32)
    part_alpha = jnp.dot(scaled, w_alpha, preferred_element_type=jnp.float32)
    part_beta = jnp.dot(scaled, w_beta, preferred_element_type=jnp.float32)
    sum_query, sum_key, sum_value, sum_gate, sum_alpha, sum_beta, own_squares = in_one_piece(
        (
            part_query.astype(jnp.bfloat16),
            part_key.astype(jnp.bfloat16),
            part_value.astype(jnp.bfloat16),
            part_gate.astype(jnp.bfloat16),
            part_alpha.astype(jnp.bfloat16),
            part_beta.astype(jnp.bfloat16),
            squares.astype(jnp.bfloat16),
        ),
        KV,
        0,
        1,
    )
    rstd = lax.rsqrt(own_squares / D + epsilon)[:, None]
    queries = (sum_query * rstd).astype(jnp.bfloat16)
    key_rows = (sum_key * rstd).astype(jnp.bfloat16)
    value_rows = (sum_value * rstd).astype(jnp.bfloat16)
    outgate = (sum_gate * rstd).astype(jnp.bfloat16)
    alphas = lax.dynamic_slice_in_dim(sum_alpha * rstd, tp_place * heads_dev, heads_dev, 1)
    beta_pre = lax.dynamic_slice_in_dim(sum_beta * rstd, tp_place * heads_dev, heads_dev, 1)
    own_lengths = lax.dynamic_slice_in_dim(lengths, kv_place * seq_dev, seq_dev)
    live = jnp.arange(NEW, dtype=jnp.int32)[None, :] < own_lengths[:, None]
    query_h = unit_rows(queries.astype(jnp.float32).reshape(seq_dev, NEW, heads_dev, DK)) * DK ** (
        -0.5
    )
    key_h = unit_rows(key_rows.astype(jnp.float32).reshape(seq_dev, NEW, heads_dev, DK))
    value_h = value_rows.astype(jnp.float32).reshape(seq_dev, NEW, heads_dev, DV)
    decays = -jnp.exp(decay_log) * jax.nn.softplus(alphas + decay_bias)
    decays = jnp.where(live[:, :, None], decays.reshape(seq_dev, NEW, heads_dev), 0.0)
    betas = jnp.where(
        live[:, :, None], jax.nn.sigmoid(beta_pre).reshape(seq_dev, NEW, heads_dev), 0.0
    )
    new_memory, attended = advance(memory, query_h, key_h, value_h, decays, betas)
    attended = attended * lax.rsqrt(jnp.mean(attended * attended, axis=-1, keepdims=True) + epsilon)
    gate_h = outgate.astype(jnp.float32).reshape(seq_dev, NEW, heads_dev, DV)
    mixed = (
        (attended * head_gain * jax.nn.silu(gate_h))
        .astype(jnp.bfloat16)
        .reshape(own_rows, heads_dev * DV)
    )
    attn_terms = jnp.dot(collect(mixed, KV, 0), w_output, preferred_element_type=jnp.float32)
    attn_total = of_everyone(attn_terms, "tp")
    hidden = (token_f + attn_total).astype(jnp.bfloat16)
    hidden_f = hidden.astype(jnp.float32)
    hidden_squares = jnp.sum(hidden_f * hidden_f, axis=1)
    hscaled = (hidden_f * mlp_gain).astype(jnp.bfloat16)
    all_live = (jnp.arange(NEW, dtype=jnp.int32)[None, :] < lengths[:, None]).reshape(total_rows)
    part_gate_rows = jnp.dot(hscaled, w_gate, preferred_element_type=jnp.float32)
    part_up_rows = jnp.dot(hscaled, w_up, preferred_element_type=jnp.float32)
    gate_rows, up_rows, mlp_squares = in_one_piece(
        (
            part_gate_rows.astype(jnp.bfloat16),
            part_up_rows.astype(jnp.bfloat16),
            hidden_squares.astype(jnp.bfloat16),
        ),
        KV,
        0,
        1,
    )
    rstd2 = lax.rsqrt(mlp_squares / D + epsilon)[:, None]
    active = (jax.nn.silu(gate_rows * rstd2) * (up_rows * rstd2)).astype(jnp.bfloat16)
    feed_terms = jnp.dot(
        gather_axes(active, KV, (0, 1), 0), w_down, preferred_element_type=jnp.float32
    )
    feed_total = over_copies(feed_terms.astype(jnp.bfloat16), "tp").astype(jnp.float32)
    layer_out = jnp.where(all_live[:, None], hidden_f + feed_total, 0.0).astype(jnp.bfloat16)
    return (layer_out, new_memory)


def solution(mesh):
    torus = Mesh(mesh.devices.reshape(16, 4, mesh.shape["tp"]), ("kv_0", "kv_1", "tp"))
    placed = (
        P(None, KV),
        P(),
        P(KV, "tp", None, None),
        P(KV),
        P(KV, "tp"),
        P(KV, "tp"),
        P(KV, "tp"),
        P(KV, "tp"),
        P(KV, None),
        P(KV, None),
        P("tp"),
        P("tp"),
        P(),
        P("tp", KV),
        P(KV),
        P(KV, "tp"),
        P(KV, "tp"),
        P("tp", KV),
    )
    return jax.shard_map(
        per_device,
        mesh=torus,
        in_specs=placed,
        out_specs=(P(None, KV), P(KV, "tp", None, None)),
        check_vma=False,
    )
```

profile of v0, /device:TPU:1, one launch (start us, length us, event | category | flops | bytes accessed | tf_op | source)
XLA Modules:
  0.0 242.6 jit_solution(11514970106353623751)
XLA Ops:
  0.7 0.8 fusion.21
  1.5 1.1 convolution_convert_fusion.5
  2.6 1.1 convolution_convert_fusion.4
  3.8 1.1 convolution_convert_fusion.3
  4.9 1.1 convolution_convert_fusion.2
  7.0 2.5 %concatenate.42 = bf16[64,4,1057]{2,1,0:T(4,128)(2,1)} concatenate(bf16[64,4,256]{2,1,0:T(4,128)(2,1)S(1)} %concatenate.36, bf16[64,4,256]{2,1,0:T(4,128)(2,1)S(1)} %concatenate.37, bf16[64,4,256]{2,1,0:T(4,128)(2,1)S(1)} %concatenate.38, bf16[64,4,256]{2,1,0:T(4,128)(2,1)S(1)} %concatenate.39, bf16[64,4,16]{2,1,0:T(4,128)(2,1)S(1)} %bitcast.169, ...), dimensions={2} | concatenate | bytes 1082368 | tf_op jit(solution)/shard_map/concatenate | solution.py:32
  9.5 19.3 %all-to-all-start = ((bf16[64,4,1057]{2,1,0:T(4,128)(2,1)}), bf16[64,4,1057]{2,1,0:T(4,128)(2,1)S(1)}, u32[]{:S(2)}, u32[]{:S(2)}) async-start(bf16[64,4,1057]{2,1,0:T(4,128)(2,1)} %concatenate.42), calls=%async_computation | async-start | bytes 1179648 | tf_op jit(solution)/shard_map/all_to_all | solution.py:26
  28.8 0.6 dynamic_slice.9
  29.4 0.6 iota_compare_fusion.1
  30.1 31.9 %all-to-all-done = bf16[64,4,1057]{2,1,0:T(4,128)(2,1)S(1)} async-done(((bf16[64,4,1057]{2,1,0:T(4,128)(2,1)}), bf16[64,4,1057]{2,1,0:T(4,128)(2,1)S(1)}, u32[]{:S(2)}, u32[]{:S(2)}) %all-to-all-start) | async-done | bytes 541216 | tf_op jit(solution)/shard_map/all_to_all | solution.py:26
  67.1 22.2 %all_to_all.25 = bf16[64,4,256]{2,1,0:T(4,128)(2,1)S(1)} all-to-all(bf16[64,4,256]{2,1,0:T(4,128)(2,1)S(1)} %broadcast_in_dim.32), channel_id=1, replica_groups=mesh['kv_0'=16,'kv_1'=4,'tp'=8] {'kv_0','kv_1'}, dimensions={0} | all-to-all | bytes 262144 | tf_op jit(solution)/shard_map/all_to_all | solution.py:44
  89.6 17.0 %all_to_all.26 = f32[8,256,64]{1,2,0:T(8,128)S(1)} all-to-all(f32[8,256,64]{1,2,0:T(8,128)S(1)} %broadcast_in_dim.33), channel_id=1, replica_groups=mesh['kv_0'=16,'kv_1'=4,'tp'=8] {'tp'}, dimensions={0} | all-to-all | bytes 1048576 | tf_op jit(solution)/shard_map/all_to_all | solution.py:44
  106.7 0.4 convolution_convert_fusion.1
  107.6 0.4 convolution_convert_fusion
  108.4 0.7 pad_maximum_fusion
  109.1 74.8 %all_to_all.27 = bf16[64,4,2817]{2,1,0:T(4,128)(2,1)S(1)} all-to-all(bf16[64,4,2817]{2,1,0:T(4,128)(2,1)S(1)} %pad_maximum_fusion), channel_id=1, replica_groups=mesh['kv_0'=16,'kv_1'=4,'tp'=8] {'kv_0','kv_1'}, dimensions={0} | all-to-all | bytes 2884608 | tf_op jit(solution)/shard_map/all_to_all | solution.py:26
  183.9 0.6 convert_reduce_fusion
  184.8 22.4 %all-gather.1 = bf16[16,4,1408]{2,1,0:T(4,128)(2,1)S(1)} all-gather(bf16[1,4,1408]{2,1,0:T(4,128)(2,1)S(1)} %fusion.47), channel_id=2, replica_groups=mesh['kv_0'=16,'kv_1'=4,'tp'=8] {'kv_0'}, dimensions={0}, use_global_device_ids=true | all-gather | bytes 191488 | tf_op jit(solution)/shard_map/all_gather | solution.py:67
  207.1 10.5 %all_gather.7 = bf16[64,4,1408]{2,1,0:T(4,128)(2,1)S(1)} all-gather(bf16[16,4,1408]{2,1,0:T(4,128)(2,1)S(1)} %all-gather.1), channel_id=1, replica_groups=mesh['kv_0'=16,'kv_1'=4,'tp'=8] {'kv_1'}, dimensions={0}, use_global_device_ids=true | all-gather | bytes 901120 | tf_op jit(solution)/shard_map/all_gather | solution.py:67
  218.1 0.5 copy-done.4
  219.0 0.7 broadcast_in_dim.35
  219.7 15.8 %all-to-all-start.4 = ((bf16[8,256,64]{1,2,0:T(8,128)(2,1)}), bf16[8,256,64]{1,2,0:T(8,128)(2,1)S(1)}, u32[]{:S(2)}, u32[]{:S(2)}) async-start(bf16[8,256,64]{1,2,0:T(8,128)(2,1)} %broadcast_in_dim.35), calls=%async_computation.4 | async-start | bytes 524288 | tf_op jit(solution)/shard_map/all_to_all | solution.py:44
  235.6 6.3 %all-to-all-done.4 = bf16[8,256,64]{1,2,0:T(8,128)(2,1)S(1)} async-done(((bf16[8,256,64]{1,2,0:T(8,128)(2,1)}), bf16[8,256,64]{1,2,0:T(8,128)(2,1)S(1)}, u32[]{:S(2)}, u32[]{:S(2)}) %all-to-all-start.4) | async-done | bytes 262176 | tf_op jit(solution)/shard_map/all_to_all | solution.py:44
  242.0 0.6 fusion.26
  (95 shorter events, 8.5 us)
Async XLA Ops:
  0.6 106.1 %copy-start = (bf16[64,1408]{1,0:T(8,128)(2,1)S(1)}, bf16[64,1408]{1,0:T(8,128)(2,1)}, u32[]{:S(2)}) copy-start(bf16[64,1408]{1,0:T(8,128)(2,1)} %param.33) | copy-start | bytes 540676
  0.6 5.4 %copy-start.2 = (bf16[256,64]{0,1:T(8,128)(2,1)S(1)}, bf16[256,64]{0,1:T(8,128)(2,1)}, u32[]{:S(2)}) copy-start(bf16[256,64]{0,1:T(8,128)(2,1)} %param.18) | copy-start | bytes 98308
  0.7 5.4 %copy-start.7 = (f32[64]{0:T(128)S(1)}, f32[64]{0:T(128)}, u32[]{:S(2)}) copy-start(f32[64]{0:T(128)} %param.21) | copy-start | bytes 772
  0.7 5.4 %copy-start.11 = (bf16[64,16]{0,1:T(8,128)(2,1)S(1)}, bf16[64,16]{0,1:T(8,128)(2,1)}, u32[]{:S(2)}) copy-start(bf16[64,16]{0,1:T(8,128)(2,1)} %param.26) | copy-start | bytes 6148
  0.7 5.7 %copy-start.12 = (bf16[64,16]{0,1:T(8,128)(2,1)S(1)}, bf16[64,16]{0,1:T(8,128)(2,1)}, u32[]{:S(2)}) copy-start(bf16[64,16]{0,1:T(8,128)(2,1)} %param.27) | copy-start | bytes 6148
  6.0 22.8 %copy-start.10 = (s32[64]{0:T(128)S(1)}, s32[64]{0:T(128)}, u32[]{:S(2)}) copy-start(s32[64]{0:T(128)} %param.19) | copy-start | bytes 772
  6.0 24.1 %copy-start.13 = (f32[2]{0:T(128)S(1)}, f32[2]{0:T(128)}, u32[]{:S(2)}) copy-start(f32[2]{0:T(128)} %param.28) | copy-start | bytes 28
  6.0 24.1 %copy-start.14 = (f32[128]{0:T(128)S(1)}, f32[128]{0:T(128)}, u32[]{:S(2)}) copy-start(f32[128]{0:T(128)} %param.30) | copy-start | bytes 1540
  7.0 55.6 %copy-start.9 = (f32[2]{0:T(128)S(1)}, f32[2]{0:T(128)}, u32[]{:S(2)}) copy-start(f32[2]{0:T(128)} %param.29) | copy-start | bytes 28
  7.0 56.8 %copy-start.1 = (f32[1,2,128,128]{3,2,1,0:T(8,128)S(1)}, f32[1,2,128,128]{3,2,1,0:T(8,128)}, u32[]{:S(2)}) copy-start(f32[1,2,128,128]{3,2,1,0:T(8,128)} %param.20) | copy-start | bytes 393220
  9.5 52.5 %all-to-all-start = ((bf16[64,4,1057]{2,1,0:T(4,128)(2,1)}), bf16[64,4,1057]{2,1,0:T(4,128)(2,1)S(1)}, u32[]{:S(2)}, u32[]{:S(2)}) async-start(bf16[64,4,1057]{2,1,0:T(4,128)(2,1)} %concatenate.42), calls=%async_computation | async-start | bytes 1179648 | tf_op jit(solution)/shard_map/all_to_all | solution.py:26
  30.1 59.3 %copy-start.6 = (bf16[256,64]{0,1:T(8,128)(2,1)S(1)}, bf16[256,64]{0,1:T(8,128)(2,1)}, u32[]{:S(2)}) copy-start(bf16[256,64]{0,1:T(8,128)(2,1)} %param.31) | copy-start | bytes 98308
  66.5 40.1 %copy-start.3 = (f32[1,2,128,128]{3,2,1,0:T(8,128)}, f32[1,2,128,128]{3,2,1,0:T(8,128)S(1)}, u32[]{:S(2)}) copy-start(f32[1,2,128,128]{3,2,1,0:T(8,128)S(1)} %multiply_add_fusion) | copy-start | bytes 393220
  67.1 39.6 %copy-start.8 = (f32[64]{0:T(128)S(1)}, f32[64]{0:T(128)}, u32[]{:S(2)}) copy-start(f32[64]{0:T(128)} %param.32) | copy-start | bytes 772
  106.6 0.9 copy-start.5
  217.7 0.9 copy-start.4
  219.7 22.3 %all-to-all-start.4 = ((bf16[8,256,64]{1,2,0:T(8,128)(2,1)}), bf16[8,256,64]{1,2,0:T(8,128)(2,1)S(1)}, u32[]{:S(2)}, u32[]{:S(2)}) async-start(bf16[8,256,64]{1,2,0:T(8,128)(2,1)} %broadcast_in_dim.35), calls=%async_computation.4 | async-start | bytes 524288 | tf_op jit(solution)/shard_map/all_to_all | solution.py:44
where the time goes:
time: 243 us
  blocking collectives  147 us (60%)
  waiting for transfers between devices  38.2 us (16%)
  starting transfers between devices  35 us (14%)
  matrix products  8.38 us (3%)
  local copies, waits for them, and re-layouts  7.27 us (3%)
  other arithmetic  5.71 us (2%)
    all_to_all x1, blocking collectives, sent_and_summed(): lax.all_to_all(parts, axis, split_axis=0, concat_axis=0, tiled=True)  74.8 us
    all_to_all x2, blocking collectives, copy_for_each(): lax.all_to_all(jnp.broadcast_to(shard[None], (peers, *shard.shape)), axis...  39.2 us
    all_gather x2, blocking collectives, gather_in_order(): parts = lax.all_gather(parts, axes[k], axis=0, tiled=True)  32.9 us
    all_to_all x1, waiting for transfers between devices, sent_and_summed(): lax.all_to_all(parts, axis, split_axis=0, concat_axis=0, tiled=True)  31.9 us
    all_to_all x1, starting transfers between devices, sent_and_summed(): lax.all_to_all(parts, axis, split_axis=0, concat_axis=0, tiled=True)  19.3 us
    all_to_all x1, starting transfers between devices, copy_for_each(): lax.all_to_all(jnp.broadcast_to(shard[None], (peers, *shard.shape)), axis...  15.8 us
    all_to_all x1, waiting for transfers between devices, copy_for_each(): lax.all_to_all(jnp.broadcast_to(shard[None], (peers, *shard.shape)), axis...  6.3 us
  transfers between devices with their start and end apart: 2, of which 2 were waited for; matrix products, arithmetic and copies ran while one was open for 1% of the time, Pallas kernels for 0%

commit v1 on v0

v1 whole, which is shorter than its diff:
```python
import jax
import jax.numpy as jnp
from jax import lax
from jax.experimental import pallas as pl
from jax.experimental.pallas import tpu as pltpu
from jax.sharding import PartitionSpec as P

MESH = pl.DeviceIdType.MESH
F32, BF16, I32 = jnp.float32, jnp.bfloat16, jnp.int32
D, DK, NEW, SEQS = 4096, 128, 4, 64
Z, Y, TP = 16, 4, 8
ROWS = SEQS * NEW
PLACES = 8 * Z
EPS = 1e-06
W1 = 640
FFY = 352
FP = 384
W2 = 2 * FP
PH = 13
S_Y, S_Z, S_M, S_C, S_H, S_G, S_A, S_F, S_O, S_WO, S_WG, S_WD, S_GN = range(PH)


def iota(shape, dim):
    return lax.broadcasted_iota(I32, shape, dim)


def mm(a, b):
    return jnp.dot(a, b, preferred_element_type=F32)


def kernel(
    tok_ref, lens_ref, lencol_ref, mem_ref, ngain_ref, wq_ref, wk_ref, wv_ref, wg_ref, wa_ref, wb_ref,
    dlog_ref, dbias_ref, hgain_ref, wout_ref, mgain_ref, wgate_ref, wup_ref, wdown_ref,
    out_ref, nmem_ref,
    part, yrecv, zs1, zr1, mrecv, cs, cr, hbuf, wgs, wgr, wob, wdb, gl, gb, zs2, zr2, ab, fs, fr, ob, hct, wab,
    send, recv,
):
    kv = lax.axis_index("kv")
    tp = lax.axis_index("tp")
    z = kv // Y
    y = kv % Y
    group = y * TP + tp

    def y_peer(k):
        return z * Y + (y + k) % Y

    def z_peer(j):
        away = 8 - (j + 1) // 2
        return (z + Z + away * (2 * (j % 2) - 1)) % Z

    barrier = pltpu.get_barrier_semaphore()

    def greet_group(j, c):
        other = (group + j) % (Y * TP)
        pl.semaphore_signal(barrier, inc=1, device_id=(z * Y + other // TP, other % TP), device_id_type=MESH)
        return c

    def greet_z(j, c):
        pl.semaphore_signal(barrier, inc=1, device_id=(z_peer(j) * Y + y, tp), device_id_type=MESH)
        return c

    lax.fori_loop(0, Z - 1, greet_z, 0)
    lax.fori_loop(1, Y * TP, greet_group, 0)

    def rcopy(src, dst, phase, where):
        return pltpu.make_async_remote_copy(
            src_ref=src, dst_ref=dst, send_sem=send.at[phase], recv_sem=recv.at[phase],
            device_id=where, device_id_type=MESH,
        )

    def arrived(ref, phase):
        rcopy(ref, ref, phase, (y_peer(1), tp)).wait_recv()

    def sent(ref, phase):
        rcopy(ref, ref, phase, (y_peer(1), tp)).wait_send()

    tok_f = tok_ref[...].astype(F32)
    tok_b = tok_ref[...]
    scaled = (tok_f * ngain_ref[...]).astype(BF16)
    at = iota((2 * ROWS, ROWS), 0)
    row = iota((2 * ROWS, ROWS), 1)
    wanted = 16 * ((at >> 3) & 15) + 4 * (at >> 7) + (at & 3)
    turn = jnp.where(row == wanted, 1.0, 0.0).astype(BF16)
    xs = mm(turn, scaled).astype(BF16)
    xt = mm(turn, tok_b)
    wab[...] = jnp.zeros((64, 128), BF16)
    wab[:, 64:80] = wa_ref[...]
    wab[:, 80:96] = wb_ref[...]
    squares = jnp.sum(xt * xt, axis=1, keepdims=True)
    high = squares.astype(BF16).astype(F32)
    low = squares - high
    eye = jnp.where(iota((64, 128), 0) == iota((64, 128), 1), 1.0, 0.0).astype(BF16)
    lane = iota((2 * ROWS, 128), 1)
    extra = mm(xs, wab[...]) + mm(xt.astype(BF16), eye)
    extra = jnp.where(lane == 96, high, jnp.where(lane == 97, low, extra))
    second = (iota((2 * ROWS, 256), 0) & 4) == 4
    left = jnp.where(second, mm(xs, wv_ref[...]), mm(xs, wq_ref[...]))
    part[:, :, :, 0:256] = left.reshape(Y, Z, 8, 256).astype(BF16)
    right = jnp.where(second, mm(xs, wg_ref[...]), mm(xs, wk_ref[...]))
    part[:, :, :, 256:512] = right.reshape(Y, Z, 8, 256).astype(BF16)
    part[:, :, :, 512:640] = extra.reshape(Y, Z, 8, 128).astype(BF16)

    for k in range(Y):
        wgs[k, :, 0:FFY] = wgate_ref[:, FFY * k : FFY * (k + 1)]
        wgs[k, :, FFY:FP] = jnp.zeros((64, FP - FFY), BF16)
        wgs[k, :, FP : FP + FFY] = wup_ref[:, FFY * k : FFY * (k + 1)]
        wgs[k, :, FP + FFY : W2] = jnp.zeros((64, FP - FFY), BF16)
        wdb[k, FFY:FP, :] = jnp.zeros((FP - FFY, 64), BF16)
    gl[...] = jnp.zeros((8, 128), F32) + jnp.concatenate([mgain_ref[...], mgain_ref[...]], axis=1)

    pl.semaphore_wait(barrier, Z - 1 + Y * TP - 1)

    for k in range(1, Y):
        peer = y_peer(k)
        rcopy(part.at[peer % Y], yrecv.at[y], S_Y, (peer, tp)).start()
    for k in range(1, Y):
        peer = y_peer(k)
        rcopy(wout_ref, wob.at[y], S_WO, (peer, tp)).start()
        rcopy(wgs.at[peer % Y], wgr.at[y], S_WG, (peer, tp)).start()
        rcopy(
            wdown_ref.at[pl.ds(pl.multiple_of((peer % Y) * FFY, 16), FFY)], wdb.at[y, pl.ds(0, FFY)], S_WD, (peer, tp)
        ).start()
        rcopy(gl, gb.at[y], S_GN, (peer, tp)).start()

    yrecv[y] = part[y]
    wob[y] = wout_ref[...]
    wgr[y] = wgs[y]
    wdb[y, 0:FFY, :] = wdown_ref[pl.ds(pl.multiple_of(y * FFY, 16), FFY), :]
    gb[y] = gl[...]

    seq = iota((SEQS, ROWS), 0)
    lens = lencol_ref[...] + jnp.zeros((SEQS, ROWS), I32)
    place = iota((PLACES, ROWS), 0)

    def chooser(seq_of, slot):
        mine = jnp.sum(jnp.where(seq == seq_of, lens, 0), axis=0, keepdims=True)
        before = jnp.sum(jnp.where(seq < seq_of, lens, 0), axis=0, keepdims=True)
        slot = slot[0:1]
        index = before + slot
        chunk = (index * 9363) >> 16
        goes = jnp.where(slot < mine, index + chunk, -1)
        return jnp.where(place == goes, 1.0, 0.0).astype(BF16)

    col = iota((SEQS, ROWS), 1)
    pick = chooser(4 * ((col >> 2) & 15) + (col >> 6), col & 3)
    give = chooser(col >> 2, col & 3)

    arrived(yrecv.at[0:3], S_Y)
    total = yrecv[0].astype(F32)
    for k in range(1, Y):
        total = total + yrecv[k].astype(F32)
    zs1[...] = total.astype(BF16)

    def send_z1(j, c):
        to = z_peer(j)
        rcopy(zs1.at[to], zr1.at[z], S_Z, (to * Y + y, tp)).start()
        return c

    lax.fori_loop(0, Z - 1, send_z1, 0)
    zr1[z] = zs1[z]
    arrived(zr1.at[0 : Z - 1], S_Z)

    mine = jnp.sum(zr1[...].astype(F32), axis=0)
    lane8 = iota((8, 128), 1)
    ext = mine[:, 512:640]

    def lane_of(values, where):
        return jnp.sum(jnp.where(lane8 == where, values, 0.0), axis=1, keepdims=True)

    rstd = lax.rsqrt((lane_of(ext, 96) + lane_of(ext, 97)) / D + EPS)
    main = (mine[:, 0:512] * rstd).astype(BF16).astype(F32)
    ext = ext * rstd
    live = iota((8, 1), 0) < lens_ref[kv]
    rows = []
    for h in range(2):
        alpha = lane_of(ext, 64 + 2 * tp + h)
        beta = jax.nn.sigmoid(lane_of(ext, 80 + 2 * tp + h))
        shifted = alpha + dbias_ref[0, h]
        soft = jnp.maximum(shifted, 0.0) + jnp.log1p(jnp.exp(-jnp.abs(shifted)))
        rate = jnp.exp(jnp.zeros((8, 1), F32) + dlog_ref[0, h])
        decay = jnp.exp(jnp.where(live, -rate * soft, 0.0))
        beta = jnp.where(live, beta, 0.0)
        q8 = main[:, 128 * h : 128 * h + 128]
        k8 = main[:, 256 + 128 * h : 384 + 128 * h]
        q8 = q8 * lax.rsqrt(jnp.sum(q8 * q8, axis=1, keepdims=True) + EPS) * DK**-0.5
        k8 = k8 * lax.rsqrt(jnp.sum(k8 * k8, axis=1, keepdims=True) + EPS)
        qt, kt = q8.T, k8.T
        memory = mem_ref[0, h]
        for t in range(NEW):
            kcol = kt[:, t : t + 1]
            memory = memory * decay[t : t + 1]
            guess = jnp.sum(memory * kcol, axis=0, keepdims=True)
            fix = beta[t : t + 1] * (main[4 + t : 5 + t, 128 * h : 128 * h + 128] - guess)
            memory = memory + kcol * fix
            rows.append(jnp.sum(memory * qt[:, t : t + 1], axis=0, keepdims=True))
        nmem_ref[0, h] = memory
    attended = jnp.concatenate(rows, axis=0)
    attended = attended * lax.rsqrt(jnp.mean(attended * attended, axis=1, keepdims=True) + EPS)
    gates = jnp.concatenate([main[4:8, 256:384], main[4:8, 384:512]], axis=0)
    mixed = attended * hgain_ref[...] * (gates * jax.nn.sigmoid(gates))
    mrecv[z] = mixed.astype(BF16)

    def send_m(j, c):
        rcopy(mrecv.at[z], mrecv.at[z], S_M, (z_peer(j) * Y + y, tp)).start()
        return c

    lax.fori_loop(0, Z - 1, send_m, 0)
    arrived(wob.at[0:3], S_WO)
    wo = jnp.concatenate([wob[k].astype(F32) for k in range(Y)], axis=1).astype(BF16)
    arrived(gb.at[0:3], S_GN)
    low_lane = iota((1, 128), 1) < 64
    gain = jnp.concatenate(
        [jnp.where(low_lane, gb[0, 0:1], gb[1, 0:1]), jnp.where(low_lane, gb[2, 0:1], gb[3, 0:1])], axis=1
    )
    low_half = iota((8, 128), 0) < 4

    def kept(k):
        return jnp.where(
            low_half, yrecv[k, 2 * tp, :, 512:640].astype(F32), yrecv[k, 2 * tp + 1, :, 512:640].astype(F32)
        )

    residual = jnp.concatenate(
        [
            jnp.where(low_lane, kept(0), pltpu.roll(kept(1), 64, 1)),
            jnp.where(low_lane, kept(2), pltpu.roll(kept(3), 64, 1)),
        ],
        axis=1,
    )
    arrived(mrecv.at[0 : Z - 1], S_M)

    heads = mrecv[...].astype(F32).reshape(8 * Z, 128).astype(BF16)
    first_head = (iota((8 * Z, 256), 0) & 4) == 0
    terms = jnp.where(first_head, mm(heads, wo[0:128]), mm(heads, wo[128:256]))
    terms = terms.reshape(TP, 2, 8, 256)
    even, odd = terms[:, 0], terms[:, 1]
    even = even + jnp.concatenate([even[:, 4:8], even[:, 0:4]], axis=1)
    odd = odd + jnp.concatenate([odd[:, 4:8], odd[:, 0:4]], axis=1)
    cs[...] = jnp.where((iota((TP, 8, 256), 1) & 4) == 0, even, odd)

    def send_c(j, c):
        to = (tp + j) % TP
        rcopy(cs.at[to], cr.at[tp], S_C, (kv, to)).start()
        return c

    lax.fori_loop(1, TP, send_c, 0)
    cr[tp] = cs[tp]
    arrived(cr.at[0 : TP - 1], S_C)
    hbuf[group] = (residual + jnp.sum(cr[...], axis=0)).astype(BF16)

    def send_h(j, c):
        other = (group + j) % (Y * TP)
        rcopy(hbuf.at[group], hbuf.at[group], S_H, (z * Y + other // TP, other % TP)).start()
        return c

    lax.fori_loop(1, Y * TP, send_h, 0)
    arrived(wgr.at[0:3], S_WG)
    arrived(hbuf.at[0 : Y * TP - 1], S_H)

    hidden = mm(pick, hbuf[...].astype(F32).reshape(ROWS, 256).astype(BF16))
    hscaled = (hidden * gain).astype(BF16)
    products = mm(hscaled, wgr[...].reshape(256, W2))
    squares2 = jnp.sum(hidden * hidden, axis=1, keepdims=True)
    high2 = squares2.astype(BF16).astype(F32)
    low2 = squares2 - high2
    lane2 = iota((PLACES, W2), 1)
    products = jnp.where(lane2 == FFY, high2, jnp.where(lane2 == FFY + 1, low2, products))
    zs2[...] = products.reshape(Z, 8, W2).astype(BF16)

    def send_g(j, c):
        to = z_peer(j)
        rcopy(zs2.at[to], zr2.at[z], S_G, (to * Y + y, tp)).start()
        return c

    lax.fori_loop(0, Z - 1, send_g, 0)
    zr2[z] = zs2[z]
    hct[...] = hidden.T
    arrived(wdb.at[0:3, 0:FFY], S_WD)
    arrived(zr2.at[0 : Z - 1], S_G)
    summed = jnp.sum(zr2[...].astype(F32), axis=0)
    lane3 = iota((8, FP), 1)
    gate, up = summed[:, 0:FP], summed[:, FP:W2]
    total2 = jnp.sum(jnp.where((lane3 == FFY) | (lane3 == FFY + 1), gate, 0.0), axis=1, keepdims=True)
    rstd2 = lax.rsqrt(total2 / D + EPS)
    gate = jnp.where(lane3 < FFY, gate, 0.0) * rstd2
    ab[z] = (gate * jax.nn.sigmoid(gate) * (up * rstd2)).astype(BF16)

    def send_a(j, c):
        rcopy(ab.at[z], ab.at[z], S_A, (z_peer(j) * Y + y, tp)).start()
        return c

    lax.fori_loop(0, Z - 1, send_a, 0)
    arrived(ab.at[0 : Z - 1], S_A)

    active = ab[...].astype(F32).reshape(PLACES, FP).astype(BF16)
    for k in range(Y):
        fed = lax.dot_general(wdb[k], active, (((0,), (1,)), ((), ())), preferred_element_type=F32)
        fs[TP * k : TP * (k + 1)] = fed.reshape(TP, 8, 128)

    def send_f(j, c):
        other = (group + j) % (Y * TP)
        rcopy(fs.at[other], fr.at[group], S_F, (z * Y + other // TP, other % TP)).start()
        return c

    lax.fori_loop(1, Y * TP, send_f, 0)
    fr[group] = fs[group]
    arrived(fr.at[0 : Y * TP - 1], S_F)
    ended = jnp.sum(fr[...], axis=0) + hct[pl.ds(pl.multiple_of(8 * group, 8), 8), :]
    ob[tp] = ended.astype(BF16)

    def send_o(j, c):
        rcopy(ob.at[tp], ob.at[tp], S_O, (kv, (tp + j) % TP)).start()
        return c

    lax.fori_loop(1, TP, send_o, 0)
    arrived(ob.at[0 : TP - 1], S_O)
    final = ob[...].astype(F32).reshape(64, PLACES).astype(BF16)
    out_ref[...] = lax.dot_general(give, final, (((0,), (1,)), ((), ())), preferred_element_type=F32).astype(BF16)

    for ref, phase in (
        (yrecv.at[0:3], S_Y), (zr1.at[0 : Z - 1], S_Z), (mrecv.at[0 : Z - 1], S_M), (cr.at[0 : TP - 1], S_C),
        (hbuf.at[0 : Y * TP - 1], S_H), (zr2.at[0 : Z - 1], S_G), (ab.at[0 : Z - 1], S_A),
        (fr.at[0 : Y * TP - 1], S_F), (ob.at[0 : TP - 1], S_O), (wob.at[0:3], S_WO), (wgr.at[0:3], S_WG),
        (wdb.at[0:3, 0:FFY], S_WD), (gb.at[0:3], S_GN),
    ):
        sent(ref, phase)


def per_device(
    tokens, lengths, memory, norm_gain, w_query, w_key, w_value, w_outgate, w_alpha, w_beta, decay_log, decay_bias,
    head_gain, w_output, mlp_gain, w_gate, w_up, w_down,
):
    vmem = pl.BlockSpec(memory_space=pltpu.VMEM)
    smem = pl.BlockSpec(memory_space=pltpu.SMEM)
    return tuple(
        pl.pallas_call(
            kernel,
            out_shape=(
                jax.ShapeDtypeStruct(tokens.shape, BF16),
                jax.ShapeDtypeStruct(memory.shape, F32),
            ),
            in_specs=[vmem, smem] + [vmem] * 9 + [smem, smem] + [vmem] * 6,
            out_specs=(vmem, vmem),
            scratch_shapes=[
                pltpu.VMEM((Y, Z, 8, W1), BF16),
                pltpu.VMEM((Y, Z, 8, W1), BF16),
                pltpu.VMEM((Z, 8, W1), BF16),
                pltpu.VMEM((Z, 8, W1), BF16),
                pltpu.VMEM((Z, 8, 128), BF16),
                pltpu.VMEM((TP, 8, 256), F32),
                pltpu.VMEM((TP, 8, 256), F32),
                pltpu.VMEM((Y * TP, 8, 256), BF16),
                pltpu.VMEM((Y, 64, W2), BF16),
                pltpu.VMEM((Y, 64, W2), BF16),
                pltpu.VMEM((Y, 256, 64), BF16),
                pltpu.VMEM((Y, FP, 64), BF16),
                pltpu.VMEM((8, 128), F32),
                pltpu.VMEM((Y, 8, 128), F32),
                pltpu.VMEM((Z, 8, W2), BF16),
                pltpu.VMEM((Z, 8, W2), BF16),
                pltpu.VMEM((Z, 8, FP), BF16),
                pltpu.VMEM((Y * TP, 8, 128), F32),
                pltpu.VMEM((Y * TP, 8, 128), F32),
                pltpu.VMEM((TP, 8, 128), BF16),
                pltpu.VMEM((256, 128), F32),
                pltpu.VMEM((64, 128), BF16),
                pltpu.SemaphoreType.DMA((PH,)),
                pltpu.SemaphoreType.DMA((PH,)),
            ],
            compiler_params=pltpu.CompilerParams(collective_id=0, has_side_effects=True),
        )(
            tokens, lengths, lengths[:, None], memory, norm_gain[None], w_query, w_key, w_value, w_outgate, w_alpha,
            w_beta, decay_log[None], decay_bias[None], head_gain[None], w_output, mlp_gain[None], w_gate, w_up, w_down,
        )
    )


def solution(mesh):
    kv, tp = "kv", "tp"
    placed = (
        P(None, kv), P(), P(kv, tp, None, None), P(kv), P(kv, tp), P(kv, tp), P(kv, tp), P(kv, tp), P(kv, None),
        P(kv, None), P(tp), P(tp), P(), P(tp, kv), P(kv), P(kv, tp), P(kv, tp), P(tp, kv),
    )
    return jax.shard_map(
        per_device,
        mesh=mesh,
        in_specs=placed,
        out_specs=(P(None, kv), P(kv, tp, None, None)),
        check_vma=False,
    )
```

time: 243 us -> 96 us (0.40)
  blocking collectives: 147 us -> 0 us
  Pallas kernels: 0 us -> 83.8 us
  waiting for transfers between devices: 38.2 us -> 0 us
  starting transfers between devices: 35 us -> 0 us
  matrix products: 8.38 us -> 0 us
  other arithmetic: 5.71 us -> 0 us
  local copies, waits for them, and re-layouts: 7.27 us -> 11.1 us
    all_to_all x3 -> x0, blocking collectives: 114 us -> none  [the longest x1 74.8 us: sent_and_summed(): lax.all_to_all(parts, axis, split_axis=0, concat_axis=0, tiled=True)]
    pallas_call x0 -> x1, Pallas kernels: none -> 83.8 us  [per_device(): pl.pallas_call(kernel, out_shape=(jax.ShapeDtypeStruct(tokens.shape, BF16...]
    all_to_all x2 -> x0, waiting for transfers between devices: 38.2 us -> none  [the longest x1 31.9 us: sent_and_summed(): lax.all_to_all(parts, axis, split_axis=0, concat_axis=0, tiled=True)]
    all_to_all x2 -> x0, starting transfers between devices: 35 us -> none  [the longest x1 19.3 us: sent_and_summed(): lax.all_to_all(parts, axis, split_axis=0, concat_axis=0, tiled=True)]
    all_gather x2 -> x0, blocking collectives: 32.9 us -> none  [gather_in_order(): parts = lax.all_gather(parts, axes[k], axis=0, tiled=True)]
    dot_general x18 -> x0, matrix products: 8.38 us -> none  [the longest x4 1.26 us: advance(): jnp.einsum('shde,shd->she', memory, key_rows[:, step], precision=lax.Prec...]
    unnamed x31 -> x8, local copies, waits for them, and re-layouts: 0.85 us -> 8.23 us
    concatenate x7 -> x0, local copies, waits for them, and re-layouts: 3 us -> none  [in_one_piece(): jnp.concatenate([a.reshape(*a.shape[:along], w) for a, w in zip(arrays, w...]
  transfers between devices with their start and end apart: 2 -> 0, of which waited for: 2 -> 0; matrix products, arithmetic and copies ran while one was open for 1% -> 0% of each run, Pallas kernels for 0% -> 0%
where the time goes in v1:
time: 96 us; the launch traced here: 95.6 us
  Pallas kernels  83.8 us (87%)
  local copies, waits for them, and re-layouts  11.1 us (12%)
    pallas_call x1, Pallas kernels, per_device(): pl.pallas_call(kernel, out_shape=(jax.ShapeDtypeStruct(tokens.shape, BF16...  83.8 us
    unnamed x8, local copies, waits for them, and re-layouts  8.23 us

profile of v1, /device:TPU:1, one launch (start us, length us, event | category | flops | bytes accessed | tf_op | source)
XLA Modules:
  0.0 95.6 jit_solution(1483210998864241232)
XLA Ops:
  0.6 0.0 copy-start
  0.6 1.4 %copy.22.wa_ref = bf16[64,16]{1,0:T(8,128)(2,1)} copy(bf16[64,16]{0,1:T(8,128)(2,1)} %param.26) | data formatting | bytes 4096 | tf_op args[8]
  2.0 1.4 %copy.23.wb_ref = bf16[64,16]{1,0:T(8,128)(2,1)} copy(bf16[64,16]{0,1:T(8,128)(2,1)} %param.27) | data formatting | bytes 4096 | tf_op args[9]
  3.4 1.4 %copy.21.lencol_ref = s32[64,1]{1,0:T(8,128)} copy(s32[64,1]{0,1:T(1,128)} %bitcast.6) | data formatting | bytes 512 | tf_op jit(solution)/shard_map/broadcast_in_dim | solution.py:371
  4.8 1.5 %copy.20.tok_ref = bf16[256,64]{1,0:T(8,128)(2,1)} copy(bf16[256,64]{0,1:T(8,128)(2,1)} %param.18) | data formatting | bytes 65536 | tf_op args[0]
  6.3 1.5 %copy.24.wout_ref = bf16[256,64]{1,0:T(8,128)(2,1)} copy(bf16[256,64]{0,1:T(8,128)(2,1)} %param.31) | data formatting | bytes 65536 | tf_op args[13]
  7.7 0.0 copy-done
  7.8 0.9 copy.25.wdown_ref
  8.7 83.8 %shard_map.185 = (bf16[256,64]{1,0:T(8,128)(2,1)}, f32[1,2,128,128]{3,2,1,0:T(8,128)}) custom-call(bf16[256,64]{1,0:T(8,128)(2,1)} %copy.20.tok_ref, s32[64]{0:T(128)} %lens_ref.1, s32[64,1]{1,0:T(8,128)} %copy.21.lencol_ref, f32[1,2,128,128]{3,2,1,0:T(8,128)} %mem_ref.1, f32[1,64]{1,0:T(1,128)} %bitcast.7, bf16[64,256]{1,0:T(8,128)(2,1)} %wq_ref.1, ...), custom_call_target="tpu_custom_call" | custom-call | tf_op jit(solution)/shard_map/pallas_call | solution.py:335
  92.5 1.5 %copy.26 = bf16[256,64]{0,1:T(8,128)(2,1)} copy(bf16[256,64]{1,0:T(8,128)(2,1)} %get-tuple-element.2) | data formatting | bytes 65536 | tf_op jit(solution)/shard_map/pallas_call | solution.py:335
  94.0 1.6 %copy.28 = f32[1,2,128,128]{3,2,1,0:T(8,128)} copy(f32[1,2,128,128]{3,2,1,0:T(8,128)} %get-tuple-element.7) | data formatting | bytes 262144
Async XLA Ops:
  0.6 7.1 %copy-start = (bf16[1408,64]{0,1:T(8,128)(2,1)S(1)}, bf16[1408,64]{0,1:T(8,128)(2,1)}, u32[]{:S(2)}) copy-start(bf16[1408,64]{0,1:T(8,128)(2,1)} %param.35) | copy-start | bytes 540676

commit v2 on v1

--- a/solution.py
+++ b/solution.py
@@ -28,13 +28,26 @@
     return jnp.dot(a, b, preferred_element_type=F32)
 
 
-def kernel(
-    tok_ref, lens_ref, lencol_ref, mem_ref, ngain_ref, wq_ref, wk_ref, wv_ref, wg_ref, wa_ref, wb_ref,
-    dlog_ref, dbias_ref, hgain_ref, wout_ref, mgain_ref, wgate_ref, wup_ref, wdown_ref,
-    out_ref, nmem_ref,
-    part, yrecv, zs1, zr1, mrecv, cs, cr, hbuf, wgs, wgr, wob, wdb, gl, gb, zs2, zr2, ab, fs, fr, ob, hct, wab,
-    send, recv,
-):
+IN_NAMES = 18
+
+
+def mmt(a, b):
+    return lax.dot_general(a, b, (((1,), (1,)), ((), ())), preferred_element_type=F32)
+
+
+def kernel(*refs):
+    hbm, (out_hbm, nmem_hbm) = refs[:IN_NAMES], refs[IN_NAMES : IN_NAMES + 2]
+    refs = refs[IN_NAMES + 2 :]
+    own, refs = refs[:IN_NAMES], refs[IN_NAMES:]
+    (
+        out_ref, nmem_ref,
+        part, yrecv, zs1, zr1, mrecv, cs, cr, hbuf, wgs, wgr, wob, wds, wdb, gl, gb, zs2, zr2, ab, fs, fr, ob, hct, wab,
+        send, recv, load, store,
+    ) = refs
+    (
+        tok_ref, lens_ref, mem_ref, ngain_ref, wq_ref, wk_ref, wv_ref, wg_ref, wa_ref, wb_ref,
+        dlog_ref, dbias_ref, hgain_ref, wout_ref, mgain_ref, wgate_ref, wup_ref, wdown_ref,
+    ) = own
     kv = lax.axis_index("kv")
     tp = lax.axis_index("tp")
     z = kv // Y
@@ -59,8 +72,17 @@
         pl.semaphore_signal(barrier, inc=1, device_id=(z_peer(j) * Y + y, tp), device_id_type=MESH)
         return c
 
+    loads = [pltpu.make_async_copy(hbm[k], own[k], load.at[k]) for k in range(IN_NAMES)]
+    first = (0, 3, 4, 5, 6, 7, 8, 9)
+    for k in first:
+        loads[k].start()
     lax.fori_loop(0, Z - 1, greet_z, 0)
     lax.fori_loop(1, Y * TP, greet_group, 0)
+    for k in range(IN_NAMES):
+        if k not in first:
+            loads[k].start()
+    for k in first:
+        loads[k].wait()
 
     def rcopy(src, dst, phase, where):
         return pltpu.make_async_remote_copy(
@@ -74,24 +96,21 @@
     def sent(ref, phase):
         rcopy(ref, ref, phase, (y_peer(1), tp)).wait_send()
 
-    tok_f = tok_ref[...].astype(F32)
-    tok_b = tok_ref[...]
-    scaled = (tok_f * ngain_ref[...]).astype(BF16)
     at = iota((2 * ROWS, ROWS), 0)
     row = iota((2 * ROWS, ROWS), 1)
     wanted = 16 * ((at >> 3) & 15) + 4 * (at >> 7) + (at & 3)
     turn = jnp.where(row == wanted, 1.0, 0.0).astype(BF16)
-    xs = mm(turn, scaled).astype(BF16)
-    xt = mm(turn, tok_b)
-    wab[...] = jnp.zeros((64, 128), BF16)
-    wab[:, 64:80] = wa_ref[...]
-    wab[:, 80:96] = wb_ref[...]
+    xt = mmt(turn, tok_ref[...])
+    xs = (xt * ngain_ref[...]).astype(BF16)
+    wab[...] = jnp.zeros((128, 64), BF16)
+    wab[64:80, :] = wa_ref[...]
+    wab[80:96, :] = wb_ref[...]
     squares = jnp.sum(xt * xt, axis=1, keepdims=True)
     high = squares.astype(BF16).astype(F32)
     low = squares - high
     eye = jnp.where(iota((64, 128), 0) == iota((64, 128), 1), 1.0, 0.0).astype(BF16)
     lane = iota((2 * ROWS, 128), 1)
-    extra = mm(xs, wab[...]) + mm(xt.astype(BF16), eye)
+    extra = mmt(xs, wab[...]) + mm(xt.astype(BF16), eye)
     extra = jnp.where(lane == 96, high, jnp.where(lane == 97, low, extra))
     second = (iota((2 * ROWS, 256), 0) & 4) == 4
     left = jnp.where(second, mm(xs, wv_ref[...]), mm(xs, wq_ref[...]))
@@ -100,12 +119,16 @@
     part[:, :, :, 256:512] = right.reshape(Y, Z, 8, 256).astype(BF16)
     part[:, :, :, 512:640] = extra.reshape(Y, Z, 8, 128).astype(BF16)
 
+    for k in range(IN_NAMES):
+        if k not in first:
+            loads[k].wait()
     for k in range(Y):
         wgs[k, :, 0:FFY] = wgate_ref[:, FFY * k : FFY * (k + 1)]
         wgs[k, :, FFY:FP] = jnp.zeros((64, FP - FFY), BF16)
         wgs[k, :, FP : FP + FFY] = wup_ref[:, FFY * k : FFY * (k + 1)]
         wgs[k, :, FP + FFY : W2] = jnp.zeros((64, FP - FFY), BF16)
-        wdb[k, FFY:FP, :] = jnp.zeros((FP - FFY, 64), BF16)
+        wds[k, :, 0:FFY] = wdown_ref[:, FFY * k : FFY * (k + 1)]
+        wds[k, :, FFY:FP] = jnp.zeros((64, FP - FFY), BF16)
     gl[...] = jnp.zeros((8, 128), F32) + jnp.concatenate([mgain_ref[...], mgain_ref[...]], axis=1)
 
     pl.semaphore_wait(barrier, Z - 1 + Y * TP - 1)
@@ -117,19 +140,18 @@
         peer = y_peer(k)
         rcopy(wout_ref, wob.at[y], S_WO, (peer, tp)).start()
         rcopy(wgs.at[peer % Y], wgr.at[y], S_WG, (peer, tp)).start()
-        rcopy(
-            wdown_ref.at[pl.ds(pl.multiple_of((peer % Y) * FFY, 16), FFY)], wdb.at[y, pl.ds(0, FFY)], S_WD, (peer, tp)
-        ).start()
+        rcopy(wds.at[peer % Y], wdb.at[y], S_WD, (peer, tp)).start()
         rcopy(gl, gb.at[y], S_GN, (peer, tp)).start()
 
     yrecv[y] = part[y]
     wob[y] = wout_ref[...]
     wgr[y] = wgs[y]
-    wdb[y, 0:FFY, :] = wdown_ref[pl.ds(pl.multiple_of(y * FFY, 16), FFY), :]
+    wdb[y] = wds[y]
     gb[y] = gl[...]
 
     seq = iota((SEQS, ROWS), 0)
-    lens = lencol_ref[...] + jnp.zeros((SEQS, ROWS), I32)
+    lens8 = jnp.concatenate([lens_ref[...], lens_ref[...]], axis=1).astype(F32) + jnp.zeros((8, 128), F32)
+    lens = lens8.T[0:SEQS, 0:1].astype(I32) + jnp.zeros((SEQS, ROWS), I32)
     place = iota((PLACES, ROWS), 0)
 
     def chooser(seq_of, slot):
@@ -170,14 +192,15 @@
     rstd = lax.rsqrt((lane_of(ext, 96) + lane_of(ext, 97)) / D + EPS)
     main = (mine[:, 0:512] * rstd).astype(BF16).astype(F32)
     ext = ext * rstd
-    live = iota((8, 1), 0) < lens_ref[kv]
+    length = jnp.sum(jnp.where(iota((1, SEQS), 1) == kv, lens_ref[...], 0), axis=1, keepdims=True)
+    live = iota((8, 1), 0) < length
     rows = []
     for h in range(2):
         alpha = lane_of(ext, 64 + 2 * tp + h)
         beta = jax.nn.sigmoid(lane_of(ext, 80 + 2 * tp + h))
-        shifted = alpha + dbias_ref[0, h]
+        shifted = alpha + dbias_ref[:, h : h + 1]
         soft = jnp.maximum(shifted, 0.0) + jnp.log1p(jnp.exp(-jnp.abs(shifted)))
-        rate = jnp.exp(jnp.zeros((8, 1), F32) + dlog_ref[0, h])
+        rate = jnp.exp(jnp.zeros((8, 1), F32) + dlog_ref[:, h : h + 1])
         decay = jnp.exp(jnp.where(live, -rate * soft, 0.0))
         beta = jnp.where(live, beta, 0.0)
         q8 = main[:, 128 * h : 128 * h + 128]
@@ -194,6 +217,8 @@
             memory = memory + kcol * fix
             rows.append(jnp.sum(memory * qt[:, t : t + 1], axis=0, keepdims=True))
         nmem_ref[0, h] = memory
+    keep = pltpu.make_async_copy(nmem_ref, nmem_hbm, store.at[0])
+    keep.start()
     attended = jnp.concatenate(rows, axis=0)
     attended = attended * lax.rsqrt(jnp.mean(attended * attended, axis=1, keepdims=True) + EPS)
     gates = jnp.concatenate([main[4:8, 256:384], main[4:8, 384:512]], axis=0)
@@ -206,7 +231,7 @@
 
     lax.fori_loop(0, Z - 1, send_m, 0)
     arrived(wob.at[0:3], S_WO)
-    wo = jnp.concatenate([wob[k].astype(F32) for k in range(Y)], axis=1).astype(BF16)
+    wo = wob[...].reshape(256, 256)
     arrived(gb.at[0:3], S_GN)
     low_lane = iota((1, 128), 1) < 64
     gain = jnp.concatenate(
@@ -230,7 +255,7 @@
 
     heads = mrecv[...].astype(F32).reshape(8 * Z, 128).astype(BF16)
     first_head = (iota((8 * Z, 256), 0) & 4) == 0
-    terms = jnp.where(first_head, mm(heads, wo[0:128]), mm(heads, wo[128:256]))
+    terms = jnp.where(first_head, mmt(heads, wo[:, 0:128]), mmt(heads, wo[:, 128:256]))
     terms = terms.reshape(TP, 2, 8, 256)
     even, odd = terms[:, 0], terms[:, 1]
     even = even + jnp.concatenate([even[:, 4:8], even[:, 0:4]], axis=1)
@@ -274,7 +299,7 @@
     lax.fori_loop(0, Z - 1, send_g, 0)
     zr2[z] = zs2[z]
     hct[...] = hidden.T
-    arrived(wdb.at[0:3, 0:FFY], S_WD)
+    arrived(wdb.at[0:3], S_WD)
     arrived(zr2.at[0 : Z - 1], S_G)
     summed = jnp.sum(zr2[...].astype(F32), axis=0)
     lane3 = iota((8, FP), 1)
@@ -292,9 +317,7 @@
     arrived(ab.at[0 : Z - 1], S_A)
 
     active = ab[...].astype(F32).reshape(PLACES, FP).astype(BF16)
-    for k in range(Y):
-        fed = lax.dot_general(wdb[k], active, (((0,), (1,)), ((), ())), preferred_element_type=F32)
-        fs[TP * k : TP * (k + 1)] = fed.reshape(TP, 8, 128)
+    fs[...] = mmt(wdb[...].reshape(256, FP), active).reshape(Y * TP, 8, 128)
 
     def send_f(j, c):
         other = (group + j) % (Y * TP)
@@ -314,64 +337,67 @@
     lax.fori_loop(1, TP, send_o, 0)
     arrived(ob.at[0 : TP - 1], S_O)
     final = ob[...].astype(F32).reshape(64, PLACES).astype(BF16)
-    out_ref[...] = lax.dot_general(give, final, (((0,), (1,)), ((), ())), preferred_element_type=F32).astype(BF16)
+    out_ref[...] = mm(final, give).astype(BF16)
+    result = pltpu.make_async_copy(out_ref, out_hbm, store.at[1])
+    result.start()
 
     for ref, phase in (
         (yrecv.at[0:3], S_Y), (zr1.at[0 : Z - 1], S_Z), (mrecv.at[0 : Z - 1], S_M), (cr.at[0 : TP - 1], S_C),
         (hbuf.at[0 : Y * TP - 1], S_H), (zr2.at[0 : Z - 1], S_G), (ab.at[0 : Z - 1], S_A),
         (fr.at[0 : Y * TP - 1], S_F), (ob.at[0 : TP - 1], S_O), (wob.at[0:3], S_WO), (wgr.at[0:3], S_WG),
-        (wdb.at[0:3, 0:FFY], S_WD), (gb.at[0:3], S_GN),
+        (wdb.at[0:3], S_WD), (gb.at[0:3], S_GN),
     ):
         sent(ref, phase)
+    keep.wait()
+    result.wait()
 
 
 def per_device(
     tokens, lengths, memory, norm_gain, w_query, w_key, w_value, w_outgate, w_alpha, w_beta, decay_log, decay_bias,
     head_gain, w_output, mlp_gain, w_gate, w_up, w_down,
 ):
-    vmem = pl.BlockSpec(memory_space=pltpu.VMEM)
-    smem = pl.BlockSpec(memory_space=pltpu.SMEM)
-    return tuple(
-        pl.pallas_call(
-            kernel,
-            out_shape=(
-                jax.ShapeDtypeStruct(tokens.shape, BF16),
-                jax.ShapeDtypeStruct(memory.shape, F32),
-            ),
-            in_specs=[vmem, smem] + [vmem] * 9 + [smem, smem] + [vmem] * 6,
-            out_specs=(vmem, vmem),
-            scratch_shapes=[
-                pltpu.VMEM((Y, Z, 8, W1), BF16),
-                pltpu.VMEM((Y, Z, 8, W1), BF16),
-                pltpu.VMEM((Z, 8, W1), BF16),
-                pltpu.VMEM((Z, 8, W1), BF16),
-                pltpu.VMEM((Z, 8, 128), BF16),
-                pltpu.VMEM((TP, 8, 256), F32),
-                pltpu.VMEM((TP, 8, 256), F32),
-                pltpu.VMEM((Y * TP, 8, 256), BF16),
-                pltpu.VMEM((Y, 64, W2), BF16),
-                pltpu.VMEM((Y, 64, W2), BF16),
-                pltpu.VMEM((Y, 256, 64), BF16),
-                pltpu.VMEM((Y, FP, 64), BF16),
-                pltpu.VMEM((8, 128), F32),
-                pltpu.VMEM((Y, 8, 128), F32),
-                pltpu.VMEM((Z, 8, W2), BF16),
-                pltpu.VMEM((Z, 8, W2), BF16),
-                pltpu.VMEM((Z, 8, FP), BF16),
-                pltpu.VMEM((Y * TP, 8, 128), F32),
-                pltpu.VMEM((Y * TP, 8, 128), F32),
-                pltpu.VMEM((TP, 8, 128), BF16),
-                pltpu.VMEM((256, 128), F32),
-                pltpu.VMEM((64, 128), BF16),
-                pltpu.SemaphoreType.DMA((PH,)),
-                pltpu.SemaphoreType.DMA((PH,)),
-            ],
-            compiler_params=pltpu.CompilerParams(collective_id=0, has_side_effects=True),
-        )(
-            tokens, lengths, lengths[:, None], memory, norm_gain[None], w_query, w_key, w_value, w_outgate, w_alpha,
-            w_beta, decay_log[None], decay_bias[None], head_gain[None], w_output, mlp_gain[None], w_gate, w_up, w_down,
-        )
+    inputs = (
+        tokens.T, lengths[None], memory, norm_gain[None], w_query, w_key, w_value, w_outgate, w_alpha.T, w_beta.T,
+        decay_log[None], decay_bias[None], head_gain[None], w_output.T, mlp_gain[None], w_gate, w_up, w_down.T,
     )
+    outputs = (jax.ShapeDtypeStruct((64, ROWS), BF16), jax.ShapeDtypeStruct(memory.shape, F32))
+    shapes = [((Y, Z, 8, W1), BF16)] * 2 + [((Z, 8, W1), BF16)] * 2 + [
+        ((Z, 8, 128), BF16),
+        ((TP, 8, 256), F32),
+        ((TP, 8, 256), F32),
+        ((Y * TP, 8, 256), BF16),
+        ((Y, 64, W2), BF16),
+        ((Y, 64, W2), BF16),
+        ((Y, 64, 256), BF16),
+        ((Y, 64, FP), BF16),
+        ((Y, 64, FP), BF16),
+        ((8, 128), F32),
+        ((Y, 8, 128), F32),
+        ((Z, 8, W2), BF16),
+        ((Z, 8, W2), BF16),
+        ((Z, 8, FP), BF16),
+        ((Y * TP, 8, 128), F32),
+        ((Y * TP, 8, 128), F32),
+        ((TP, 8, 128), BF16),
+        ((256, 128), F32),
+        ((128, 64), BF16),
+    ]
+    result, new_memory = pl.pallas_call(
+        kernel,
+        out_shape=outputs,
+        in_specs=[pl.BlockSpec(memory_space=pl.ANY)] * IN_NAMES,
+        out_specs=tuple([pl.BlockSpec(memory_space=pl.ANY)] * 2),
+        scratch_shapes=[pltpu.VMEM(a.shape, a.dtype) for a in inputs + outputs]
+        + [pltpu.VMEM(*shape) for shape in shapes]
+        + [
+            pltpu.SemaphoreType.DMA((PH,)),
+            pltpu.SemaphoreType.DMA((PH,)),
+            pltpu.SemaphoreType.DMA((IN_NAMES,)),
+            pltpu.SemaphoreType.DMA((2,)),
+        ],
+        compiler_params=pltpu.CompilerParams(collective_id=0, has_side_effects=True),
+    )(*inputs)
+    return (result.T, new_memory)
 
 
 def solution(mesh):

time: 96 us -> 85.9 us (0.89)
  local copies, waits for them, and re-layouts: 11.1 us -> 2.94 us
  Pallas kernels: 83.8 us -> 82.1 us
    unnamed x8 -> x2, local copies, waits for them, and re-layouts: 8.23 us -> 2.94 us
    pallas_call x1, Pallas kernels: 83.8 us -> 82.1 us  [per_device(): pl.pallas_call(kernel, out_shape=outputs, in_specs=[pl.BlockSpec(memory_s...]
    pallas_call x1 -> x0, local copies, waits for them, and re-layouts: 1.54 us -> none  [per_device(): pl.pallas_call(kernel, out_shape=(jax.ShapeDtypeStruct(tokens.shape, BF16...]
    broadcast_in_dim x1 -> x0, local copies, waits for them, and re-layouts: 1.36 us -> none  [per_device(): lengths[:, None]]
where the time goes in v2:
time: 85.9 us; the launch traced here: 85.7 us
  Pallas kernels  82.1 us (96%)
  local copies, waits for them, and re-layouts  2.94 us (3%)
    pallas_call x1, Pallas kernels, per_device(): pl.pallas_call(kernel, out_shape=outputs, in_specs=[pl.BlockSpec(memory_s...  82.1 us
    unnamed x2, local copies, waits for them, and re-layouts  2.94 us

profile of v2, /device:TPU:1, one launch (start us, length us, event | category | flops | bytes accessed | tf_op | source)
XLA Modules:
  0.0 85.7 jit_solution(4185307842744776432)
XLA Ops:
  0.6 82.1 %shard_map.185 = (bf16[64,256]{1,0:T(8,128)(2,1)}, f32[1,2,128,128]{3,2,1,0:T(8,128)}) custom-call(bf16[64,256]{1,0:T(8,128)(2,1)} %bitcast.14, s32[1,64]{1,0:T(1,128)} %bitcast.18, f32[1,2,128,128]{3,2,1,0:T(8,128)} %refs_2_.1, f32[1,64]{1,0:T(1,128)} %bitcast.19, bf16[64,256]{1,0:T(8,128)(2,1)} %refs_4_.1, bf16[64,256]{1,0:T(8,128)(2,1)} %refs_5_.1, ...), custom_call_target="tpu_custom_call" | custom-call | tf_op jit(solution)/shard_map/pallas_call | solution.py:385
  82.7 1.4 %copy.22 = bf16[256,64]{0,1:T(8,128)(2,1)} copy(bf16[256,64]{0,1:T(8,128)(2,1)} %bitcast.13) | data formatting | bytes 65536
  84.1 1.6 %copy.23 = f32[1,2,128,128]{3,2,1,0:T(8,128)} copy(f32[1,2,128,128]{3,2,1,0:T(8,128)} %get-tuple-element.9) | data formatting | bytes 262144

commit v3 on v2

--- a/solution.py
+++ b/solution.py
@@ -16,8 +16,10 @@
 FFY = 352
 FP = 384
 W2 = 2 * FP
-PH = 13
-S_Y, S_Z, S_M, S_C, S_H, S_G, S_A, S_F, S_O, S_WO, S_WG, S_WD, S_GN = range(PH)
+PH = 16
+S_Z, S_M, S_C, S_H, S_G, S_A, S_F, S_O, S_WO, S_WG, S_WD, S_GN, S_Y = range(PH - 3)
+PARTS = 4
+SLOTS = Z // PARTS
 
 
 def iota(shape, dim):
@@ -42,7 +44,7 @@
     (
         out_ref, nmem_ref,
         part, yrecv, zs1, zr1, mrecv, cs, cr, hbuf, wgs, wgr, wob, wds, wdb, gl, gb, zs2, zr2, ab, fs, fr, ob, hct, wab,
-        send, recv, load, store,
+        send, recv, load, store, known,
     ) = refs
     (
         tok_ref, lens_ref, mem_ref, ngain_ref, wq_ref, wk_ref, wv_ref, wg_ref, wa_ref, wb_ref,
@@ -68,15 +70,15 @@
         pl.semaphore_signal(barrier, inc=1, device_id=(z * Y + other // TP, other % TP), device_id_type=MESH)
         return c
 
-    def greet_z(j, c):
-        pl.semaphore_signal(barrier, inc=1, device_id=(z_peer(j) * Y + y, tp), device_id_type=MESH)
-        return c
+    def z_near(k):
+        return (((z + k + Z) % Z) * Y + y, tp)
 
     loads = [pltpu.make_async_copy(hbm[k], own[k], load.at[k]) for k in range(IN_NAMES)]
     first = (0, 3, 4, 5, 6, 7, 8, 9)
     for k in first:
         loads[k].start()
-    lax.fori_loop(0, Z - 1, greet_z, 0)
+    for k in (1, -1):
+        pl.semaphore_signal(barrier, inc=1, device_id=z_near(k), device_id_type=MESH)
     lax.fori_loop(1, Y * TP, greet_group, 0)
     for k in range(IN_NAMES):
         if k not in first:
@@ -98,7 +100,9 @@
 
     at = iota((2 * ROWS, ROWS), 0)
     row = iota((2 * ROWS, ROWS), 1)
-    wanted = 16 * ((at >> 3) & 15) + 4 * (at >> 7) + (at & 3)
+    slot = (at >> 3) & 15
+    toward = (z + Z + (8 - ((slot + 1) >> 1)) * (2 * (slot & 1) - 1)) & 15
+    wanted = 16 * toward + 4 * (at >> 7) + (at & 3)
     turn = jnp.where(row == wanted, 1.0, 0.0).astype(BF16)
     xt = mmt(turn, tok_ref[...])
     xs = (xt * ngain_ref[...]).astype(BF16)
@@ -131,11 +135,18 @@
         wds[k, :, FFY:FP] = jnp.zeros((64, FP - FFY), BF16)
     gl[...] = jnp.zeros((8, 128), F32) + jnp.concatenate([mgain_ref[...], mgain_ref[...]], axis=1)
 
-    pl.semaphore_wait(barrier, Z - 1 + Y * TP - 1)
-
-    for k in range(1, Y):
-        peer = y_peer(k)
-        rcopy(part.at[peer % Y], yrecv.at[y], S_Y, (peer, tp)).start()
+    pl.semaphore_wait(barrier, 2 + Y * TP - 1)
+
+    def tell(n):
+        for k in (1 << n, -(1 << n)):
+            pl.semaphore_signal(known.at[n], inc=1, device_id=z_near(k), device_id_type=MESH)
+
+    tell(0)
+    for c in range(PARTS):
+        some = pl.ds(SLOTS * c, SLOTS)
+        for k in range(1, Y):
+            peer = y_peer(k)
+            rcopy(part.at[peer % Y, some], yrecv.at[y, some], S_Y + c, (peer, tp)).start()
     for k in range(1, Y):
         peer = y_peer(k)
         rcopy(wout_ref, wob.at[y], S_WO, (peer, tp)).start()
@@ -143,11 +154,32 @@
         rcopy(wds.at[peer % Y], wdb.at[y], S_WD, (peer, tp)).start()
         rcopy(gl, gb.at[y], S_GN, (peer, tp)).start()
 
+    pl.semaphore_wait(known.at[0], 2)
+    tell(1)
     yrecv[y] = part[y]
     wob[y] = wout_ref[...]
     wgr[y] = wgs[y]
     wdb[y] = wds[y]
     gb[y] = gl[...]
+
+    pl.semaphore_wait(known.at[1], 2)
+    tell(2)
+
+    def send_z1(j, c):
+        to = z_peer(j)
+        rcopy(zs1.at[j], zr1.at[z], S_Z, (to * Y + y, tp)).start()
+        return c
+
+    pl.semaphore_wait(known.at[2], 2)
+    for c in range(PARTS):
+        low, high_slot = SLOTS * c, SLOTS * (c + 1)
+        arrived(yrecv.at[0:3, low:high_slot], S_Y + c)
+        total = yrecv[0, low:high_slot].astype(F32)
+        for k in range(1, Y):
+            total = total + yrecv[k, low:high_slot].astype(F32)
+        zs1[low:high_slot] = total.astype(BF16)
+        lax.fori_loop(low, min(high_slot, Z - 1), send_z1, 0)
+    zr1[z] = zs1[Z - 1]
 
     seq = iota((SEQS, ROWS), 0)
     lens8 = jnp.concatenate([lens_ref[...], lens_ref[...]], axis=1).astype(F32) + jnp.zeros((8, 128), F32)
@@ -167,19 +199,6 @@
     pick = chooser(4 * ((col >> 2) & 15) + (col >> 6), col & 3)
     give = chooser(col >> 2, col & 3)
 
-    arrived(yrecv.at[0:3], S_Y)
-    total = yrecv[0].astype(F32)
-    for k in range(1, Y):
-        total = total + yrecv[k].astype(F32)
-    zs1[...] = total.astype(BF16)
-
-    def send_z1(j, c):
-        to = z_peer(j)
-        rcopy(zs1.at[to], zr1.at[z], S_Z, (to * Y + y, tp)).start()
-        return c
-
-    lax.fori_loop(0, Z - 1, send_z1, 0)
-    zr1[z] = zs1[z]
     arrived(zr1.at[0 : Z - 1], S_Z)
 
     mine = jnp.sum(zr1[...].astype(F32), axis=0)
@@ -239,9 +258,15 @@
     )
     low_half = iota((8, 128), 0) < 4
 
+    def slot_of(where):
+        away = (where - z + Z) % Z
+        return (1 - away // 8) * (15 - 2 * away) + (away // 8) * (2 * away - 16)
+
     def kept(k):
         return jnp.where(
-            low_half, yrecv[k, 2 * tp, :, 512:640].astype(F32), yrecv[k, 2 * tp + 1, :, 512:640].astype(F32)
+            low_half,
+            yrecv[k, slot_of(2 * tp), :, 512:640].astype(F32),
+            yrecv[k, slot_of(2 * tp + 1), :, 512:640].astype(F32),
         )
 
     residual = jnp.concatenate(
@@ -260,7 +285,7 @@
     even, odd = terms[:, 0], terms[:, 1]
     even = even + jnp.concatenate([even[:, 4:8], even[:, 0:4]], axis=1)
     odd = odd + jnp.concatenate([odd[:, 4:8], odd[:, 0:4]], axis=1)
-    cs[...] = jnp.where((iota((TP, 8, 256), 1) & 4) == 0, even, odd)
+    cs[...] = jnp.where((iota((TP, 8, 256), 1) & 4) == 0, even, odd).astype(BF16)
 
     def send_c(j, c):
         to = (tp + j) % TP
@@ -270,7 +295,7 @@
     lax.fori_loop(1, TP, send_c, 0)
     cr[tp] = cs[tp]
     arrived(cr.at[0 : TP - 1], S_C)
-    hbuf[group] = (residual + jnp.sum(cr[...], axis=0)).astype(BF16)
+    hbuf[group] = (residual + jnp.sum(cr[...].astype(F32), axis=0)).astype(BF16)
 
     def send_h(j, c):
         other = (group + j) % (Y * TP)
@@ -317,7 +342,7 @@
     arrived(ab.at[0 : Z - 1], S_A)
 
     active = ab[...].astype(F32).reshape(PLACES, FP).astype(BF16)
-    fs[...] = mmt(wdb[...].reshape(256, FP), active).reshape(Y * TP, 8, 128)
+    fs[...] = mmt(wdb[...].reshape(256, FP), active).reshape(Y * TP, 8, 128).astype(BF16)
 
     def send_f(j, c):
         other = (group + j) % (Y * TP)
@@ -327,7 +352,7 @@
     lax.fori_loop(1, Y * TP, send_f, 0)
     fr[group] = fs[group]
     arrived(fr.at[0 : Y * TP - 1], S_F)
-    ended = jnp.sum(fr[...], axis=0) + hct[pl.ds(pl.multiple_of(8 * group, 8), 8), :]
+    ended = jnp.sum(fr[...].astype(F32), axis=0) + hct[pl.ds(pl.multiple_of(8 * group, 8), 8), :]
     ob[tp] = ended.astype(BF16)
 
     def send_o(j, c):
@@ -342,12 +367,14 @@
     result.start()
 
     for ref, phase in (
-        (yrecv.at[0:3], S_Y), (zr1.at[0 : Z - 1], S_Z), (mrecv.at[0 : Z - 1], S_M), (cr.at[0 : TP - 1], S_C),
+        (zr1.at[0 : Z - 1], S_Z), (mrecv.at[0 : Z - 1], S_M), (cr.at[0 : TP - 1], S_C),
         (hbuf.at[0 : Y * TP - 1], S_H), (zr2.at[0 : Z - 1], S_G), (ab.at[0 : Z - 1], S_A),
         (fr.at[0 : Y * TP - 1], S_F), (ob.at[0 : TP - 1], S_O), (wob.at[0:3], S_WO), (wgr.at[0:3], S_WG),
         (wdb.at[0:3], S_WD), (gb.at[0:3], S_GN),
     ):
         sent(ref, phase)
+    for c in range(PARTS):
+        sent(yrecv.at[0:3, 0:SLOTS], S_Y + c)
     keep.wait()
     result.wait()
 
@@ -363,8 +390,8 @@
     outputs = (jax.ShapeDtypeStruct((64, ROWS), BF16), jax.ShapeDtypeStruct(memory.shape, F32))
     shapes = [((Y, Z, 8, W1), BF16)] * 2 + [((Z, 8, W1), BF16)] * 2 + [
         ((Z, 8, 128), BF16),
-        ((TP, 8, 256), F32),
-        ((TP, 8, 256), F32),
+        ((TP, 8, 256), BF16),
+        ((TP, 8, 256), BF16),
         ((Y * TP, 8, 256), BF16),
         ((Y, 64, W2), BF16),
         ((Y, 64, W2), BF16),
@@ -376,8 +403,8 @@
         ((Z, 8, W2), BF16),
         ((Z, 8, W2), BF16),
         ((Z, 8, FP), BF16),
-        ((Y * TP, 8, 128), F32),
-        ((Y * TP, 8, 128), F32),
+        ((Y * TP, 8, 128), BF16),
+        ((Y * TP, 8, 128), BF16),
         ((TP, 8, 128), BF16),
         ((256, 128), F32),
         ((128, 64), BF16),
@@ -394,6 +421,7 @@
             pltpu.SemaphoreType.DMA((PH,)),
             pltpu.SemaphoreType.DMA((IN_NAMES,)),
             pltpu.SemaphoreType.DMA((2,)),
+            pltpu.SemaphoreType.REGULAR((3,)),
         ],
         compiler_params=pltpu.CompilerParams(collective_id=0, has_side_effects=True),
     )(*inputs)

time: 85.9 us -> 82.2 us (0.957)
  Pallas kernels: 82.1 us -> 78.3 us
    pallas_call x1, Pallas kernels: 82.1 us -> 78.3 us  [per_device(): pl.pallas_call(kernel, out_shape=outputs, in_specs=[pl.BlockSpec(memory_s...]
where the time goes in v3:
time: 82.2 us; the launch traced here: 81.9 us
  Pallas kernels  78.3 us (95%)
  local copies, waits for them, and re-layouts  2.94 us (4%)
    pallas_call x1, Pallas kernels, per_device(): pl.pallas_call(kernel, out_shape=outputs, in_specs=[pl.BlockSpec(memory_s...  78.3 us
    unnamed x2, local copies, waits for them, and re-layouts  2.94 us

profile of v3, /device:TPU:1, one launch (start us, length us, event | category | flops | bytes accessed | tf_op | source)
XLA Modules:
  0.0 81.9 jit_solution(4374289984175107966)
XLA Ops:
  0.6 78.3 %shard_map.185 = (bf16[64,256]{1,0:T(8,128)(2,1)}, f32[1,2,128,128]{3,2,1,0:T(8,128)}) custom-call(bf16[64,256]{1,0:T(8,128)(2,1)} %bitcast.14, s32[1,64]{1,0:T(1,128)} %bitcast.18, f32[1,2,128,128]{3,2,1,0:T(8,128)} %refs_2_.1, f32[1,64]{1,0:T(1,128)} %bitcast.19, bf16[64,256]{1,0:T(8,128)(2,1)} %refs_4_.1, bf16[64,256]{1,0:T(8,128)(2,1)} %refs_5_.1, ...), custom_call_target="tpu_custom_call" | custom-call | tf_op jit(solution)/shard_map/pallas_call | solution.py:412
  78.9 1.4 %copy.22 = bf16[256,64]{0,1:T(8,128)(2,1)} copy(bf16[256,64]{0,1:T(8,128)(2,1)} %bitcast.13) | data formatting | bytes 65536
  80.3 1.6 %copy.23 = f32[1,2,128,128]{3,2,1,0:T(8,128)} copy(f32[1,2,128,128]{3,2,1,0:T(8,128)} %get-tuple-element.9) | data formatting | bytes 262144

commit v4 on v3

--- a/solution.py
+++ b/solution.py
@@ -8,7 +8,7 @@
 MESH = pl.DeviceIdType.MESH
 F32, BF16, I32 = jnp.float32, jnp.bfloat16, jnp.int32
 D, DK, NEW, SEQS = 4096, 128, 4, 64
-Z, Y, TP = 16, 4, 8
+Z, Y, X, TP = 16, 4, 4, 8
 ROWS = SEQS * NEW
 PLACES = 8 * Z
 EPS = 1e-06
@@ -38,13 +38,12 @@
 
 
 def kernel(*refs):
-    hbm, (out_hbm, nmem_hbm) = refs[:IN_NAMES], refs[IN_NAMES : IN_NAMES + 2]
+    hbm, (out_ref, nmem_ref) = refs[:IN_NAMES], refs[IN_NAMES : IN_NAMES + 2]
     refs = refs[IN_NAMES + 2 :]
     own, refs = refs[:IN_NAMES], refs[IN_NAMES:]
     (
-        out_ref, nmem_ref,
         part, yrecv, zs1, zr1, mrecv, cs, cr, hbuf, wgs, wgr, wob, wds, wdb, gl, gb, zs2, zr2, ab, fs, fr, ob, hct, wab,
-        send, recv, load, store, known,
+        send, recv, load, known,
     ) = refs
     (
         tok_ref, lens_ref, mem_ref, ngain_ref, wq_ref, wk_ref, wv_ref, wg_ref, wa_ref, wb_ref,
@@ -63,12 +62,17 @@
         away = 8 - (j + 1) // 2
         return (z + Z + away * (2 * (j % 2) - 1)) % Z
 
+    def hops(d):
+        return min(d[0], Y - d[0]) + min(d[1], X - d[1])
+
+    apart = [(dy, dx, dc) for dy in range(Y) for dx in range(X) for dc in range(2)][1:]
+    apart = sorted(apart, key=hops, reverse=True)
+
+    def group_peer(d):
+        to_y, to_tp = (y + d[0]) % Y, (tp // 2 + d[1]) % X * 2 + (tp + d[2]) % 2
+        return to_y * TP + to_tp, (z * Y + to_y, to_tp)
+
     barrier = pltpu.get_barrier_semaphore()
-
-    def greet_group(j, c):
-        other = (group + j) % (Y * TP)
-        pl.semaphore_signal(barrier, inc=1, device_id=(z * Y + other // TP, other % TP), device_id_type=MESH)
-        return c
 
     def z_near(k):
         return (((z + k + Z) % Z) * Y + y, tp)
@@ -77,9 +81,10 @@
     first = (0, 3, 4, 5, 6, 7, 8, 9)
     for k in first:
         loads[k].start()
-    for k in (1, -1):
+    for k in (4, -4, 3, -3, 2, -2, 1, -1):
         pl.semaphore_signal(barrier, inc=1, device_id=z_near(k), device_id_type=MESH)
-    lax.fori_loop(1, Y * TP, greet_group, 0)
+    for d in apart:
+        pl.semaphore_signal(barrier, inc=1, device_id=group_peer(d)[1], device_id_type=MESH)
     for k in range(IN_NAMES):
         if k not in first:
             loads[k].start()
@@ -135,13 +140,10 @@
         wds[k, :, FFY:FP] = jnp.zeros((64, FP - FFY), BF16)
     gl[...] = jnp.zeros((8, 128), F32) + jnp.concatenate([mgain_ref[...], mgain_ref[...]], axis=1)
 
-    pl.semaphore_wait(barrier, 2 + Y * TP - 1)
-
-    def tell(n):
-        for k in (1 << n, -(1 << n)):
-            pl.semaphore_signal(known.at[n], inc=1, device_id=z_near(k), device_id_type=MESH)
-
-    tell(0)
+    pl.semaphore_wait(barrier, 8 + Y * TP - 1)
+
+    for k in (4, -4):
+        pl.semaphore_signal(known, inc=1, device_id=z_near(k), device_id_type=MESH)
     for c in range(PARTS):
         some = pl.ds(SLOTS * c, SLOTS)
         for k in range(1, Y):
@@ -154,23 +156,18 @@
         rcopy(wds.at[peer % Y], wdb.at[y], S_WD, (peer, tp)).start()
         rcopy(gl, gb.at[y], S_GN, (peer, tp)).start()
 
-    pl.semaphore_wait(known.at[0], 2)
-    tell(1)
     yrecv[y] = part[y]
     wob[y] = wout_ref[...]
     wgr[y] = wgs[y]
     wdb[y] = wds[y]
     gb[y] = gl[...]
 
-    pl.semaphore_wait(known.at[1], 2)
-    tell(2)
-
     def send_z1(j, c):
         to = z_peer(j)
         rcopy(zs1.at[j], zr1.at[z], S_Z, (to * Y + y, tp)).start()
         return c
 
-    pl.semaphore_wait(known.at[2], 2)
+    pl.semaphore_wait(known, 2)
     for c in range(PARTS):
         low, high_slot = SLOTS * c, SLOTS * (c + 1)
         arrived(yrecv.at[0:3, low:high_slot], S_Y + c)
@@ -178,7 +175,7 @@
         for k in range(1, Y):
             total = total + yrecv[k, low:high_slot].astype(F32)
         zs1[low:high_slot] = total.astype(BF16)
-        lax.fori_loop(low, min(high_slot, Z - 1), send_z1, 0)
+        lax.fori_loop(low, min(high_slot, Z - 1), send_z1, 0, unroll=True)
     zr1[z] = zs1[Z - 1]
 
     seq = iota((SEQS, ROWS), 0)
@@ -236,8 +233,6 @@
             memory = memory + kcol * fix
             rows.append(jnp.sum(memory * qt[:, t : t + 1], axis=0, keepdims=True))
         nmem_ref[0, h] = memory
-    keep = pltpu.make_async_copy(nmem_ref, nmem_hbm, store.at[0])
-    keep.start()
     attended = jnp.concatenate(rows, axis=0)
     attended = attended * lax.rsqrt(jnp.mean(attended * attended, axis=1, keepdims=True) + EPS)
     gates = jnp.concatenate([main[4:8, 256:384], main[4:8, 384:512]], axis=0)
@@ -248,7 +243,7 @@
         rcopy(mrecv.at[z], mrecv.at[z], S_M, (z_peer(j) * Y + y, tp)).start()
         return c
 
-    lax.fori_loop(0, Z - 1, send_m, 0)
+    lax.fori_loop(0, Z - 1, send_m, 0, unroll=True)
     arrived(wob.at[0:3], S_WO)
     wo = wob[...].reshape(256, 256)
     arrived(gb.at[0:3], S_GN)
@@ -287,22 +282,17 @@
     odd = odd + jnp.concatenate([odd[:, 4:8], odd[:, 0:4]], axis=1)
     cs[...] = jnp.where((iota((TP, 8, 256), 1) & 4) == 0, even, odd).astype(BF16)
 
-    def send_c(j, c):
-        to = (tp + j) % TP
-        rcopy(cs.at[to], cr.at[tp], S_C, (kv, to)).start()
-        return c
-
-    lax.fori_loop(1, TP, send_c, 0)
+    for d in apart:
+        if d[0] == 0:
+            other, where = group_peer(d)
+            rcopy(cs.at[where[1]], cr.at[tp], S_C, where).start()
     cr[tp] = cs[tp]
     arrived(cr.at[0 : TP - 1], S_C)
     hbuf[group] = (residual + jnp.sum(cr[...].astype(F32), axis=0)).astype(BF16)
 
-    def send_h(j, c):
-        other = (group + j) % (Y * TP)
-        rcopy(hbuf.at[group], hbuf.at[group], S_H, (z * Y + other // TP, other % TP)).start()
-        return c
-
-    lax.fori_loop(1, Y * TP, send_h, 0)
+    for d in apart:
+        other, where = group_peer(d)
+        rcopy(hbuf.at[group], hbuf.at[group], S_H, where).start()
     arrived(wgr.at[0:3], S_WG)
     arrived(hbuf.at[0 : Y * TP - 1], S_H)
 
@@ -321,7 +311,7 @@
         rcopy(zs2.at[to], zr2.at[z], S_G, (to * Y + y, tp)).start()
         return c
 
-    lax.fori_loop(0, Z - 1, send_g, 0)
+    lax.fori_loop(0, Z - 1, send_g, 0, unroll=True)
     zr2[z] = zs2[z]
     hct[...] = hidden.T
     arrived(wdb.at[0:3], S_WD)
@@ -338,33 +328,27 @@
         rcopy(ab.at[z], ab.at[z], S_A, (z_peer(j) * Y + y, tp)).start()
         return c
 
-    lax.fori_loop(0, Z - 1, send_a, 0)
+    lax.fori_loop(0, Z - 1, send_a, 0, unroll=True)
     arrived(ab.at[0 : Z - 1], S_A)
 
     active = ab[...].astype(F32).reshape(PLACES, FP).astype(BF16)
     fs[...] = mmt(wdb[...].reshape(256, FP), active).reshape(Y * TP, 8, 128).astype(BF16)
 
-    def send_f(j, c):
-        other = (group + j) % (Y * TP)
-        rcopy(fs.at[other], fr.at[group], S_F, (z * Y + other // TP, other % TP)).start()
-        return c
-
-    lax.fori_loop(1, Y * TP, send_f, 0)
+    for d in apart:
+        other, where = group_peer(d)
+        rcopy(fs.at[other], fr.at[group], S_F, where).start()
     fr[group] = fs[group]
     arrived(fr.at[0 : Y * TP - 1], S_F)
     ended = jnp.sum(fr[...].astype(F32), axis=0) + hct[pl.ds(pl.multiple_of(8 * group, 8), 8), :]
     ob[tp] = ended.astype(BF16)
 
-    def send_o(j, c):
-        rcopy(ob.at[tp], ob.at[tp], S_O, (kv, (tp + j) % TP)).start()
-        return c
-
-    lax.fori_loop(1, TP, send_o, 0)
+    for d in apart:
+        if d[0] == 0:
+            other, where = group_peer(d)
+            rcopy(ob.at[tp], ob.at[tp], S_O, where).start()
     arrived(ob.at[0 : TP - 1], S_O)
     final = ob[...].astype(F32).reshape(64, PLACES).astype(BF16)
     out_ref[...] = mm(final, give).astype(BF16)
-    result = pltpu.make_async_copy(out_ref, out_hbm, store.at[1])
-    result.start()
 
     for ref, phase in (
         (zr1.at[0 : Z - 1], S_Z), (mrecv.at[0 : Z - 1], S_M), (cr.at[0 : TP - 1], S_C),
@@ -375,8 +359,11 @@
         sent(ref, phase)
     for c in range(PARTS):
         sent(yrecv.at[0:3, 0:SLOTS], S_Y + c)
-    keep.wait()
-    result.wait()
+
+
+def deliver(result_ref, memory_ref, out_ref, new_ref):
+    out_ref[...] = result_ref[...]
+    new_ref[...] = memory_ref[...]
 
 
 def per_device(
@@ -411,20 +398,24 @@
     ]
     result, new_memory = pl.pallas_call(
         kernel,
-        out_shape=outputs,
+        out_shape=tuple(pltpu.VMEM(a.shape, a.dtype) for a in outputs),
         in_specs=[pl.BlockSpec(memory_space=pl.ANY)] * IN_NAMES,
-        out_specs=tuple([pl.BlockSpec(memory_space=pl.ANY)] * 2),
-        scratch_shapes=[pltpu.VMEM(a.shape, a.dtype) for a in inputs + outputs]
+        out_specs=tuple([pl.BlockSpec(memory_space=pltpu.VMEM)] * 2),
+        scratch_shapes=[pltpu.VMEM(a.shape, a.dtype) for a in inputs]
         + [pltpu.VMEM(*shape) for shape in shapes]
         + [
             pltpu.SemaphoreType.DMA((PH,)),
             pltpu.SemaphoreType.DMA((PH,)),
             pltpu.SemaphoreType.DMA((IN_NAMES,)),
-            pltpu.SemaphoreType.DMA((2,)),
-            pltpu.SemaphoreType.REGULAR((3,)),
+            pltpu.SemaphoreType.REGULAR,
         ],
         compiler_params=pltpu.CompilerParams(collective_id=0, has_side_effects=True),
     )(*inputs)
+    vmem = pl.BlockSpec(memory_space=pltpu.VMEM)
+    result, new_memory = pl.pallas_call(deliver, out_shape=outputs, in_specs=[vmem, vmem])(
+        pltpu.with_memory_space_constraint(result, pltpu.VMEM),
+        pltpu.with_memory_space_constraint(new_memory, pltpu.VMEM),
+    )
     return (result.T, new_memory)
 
 

time: 82.2 us -> 77.9 us (0.948)
  local copies, waits for them, and re-layouts: 2.94 us -> 0 us
  Pallas kernels: 78.3 us -> 77.1 us
    unnamed x2 -> x0, local copies, waits for them, and re-layouts: 2.94 us -> none
    pallas_call x1 -> x2, Pallas kernels: 78.3 us -> 77.1 us  [the longest x1 76.4 us: per_device(): pl.pallas_call(kernel, out_shape=tuple((pltpu.VMEM(a.shape, a.dtype) for...]
where the time goes in v4:
time: 77.9 us; the launch traced here: 77.7 us
  Pallas kernels  77.1 us (99%)
    pallas_call x1, Pallas kernels, per_device(): pl.pallas_call(kernel, out_shape=tuple((pltpu.VMEM(a.shape, a.dtype) for...  76.4 us

profile of v4, /device:TPU:1, one launch (start us, length us, event | category | flops | bytes accessed | tf_op | source)
XLA Modules:
  0.0 77.7 jit_solution(167690280787695707)
XLA Ops:
  0.6 76.4 %shard_map.185 = (bf16[64,256]{1,0:T(8,128)(2,1)S(1)}, f32[1,2,128,128]{3,2,1,0:T(8,128)S(1)}) custom-call(bf16[64,256]{1,0:T(8,128)(2,1)} %bitcast.13, s32[1,64]{1,0:T(1,128)} %bitcast.17, f32[1,2,128,128]{3,2,1,0:T(8,128)} %refs_2_.1, f32[1,64]{1,0:T(1,128)} %bitcast.18, bf16[64,256]{1,0:T(8,128)(2,1)} %refs_4_.1, bf16[64,256]{1,0:T(8,128)(2,1)} %refs_5_.1, ...), custom_call_target="tpu_custom_call" | custom-call | tf_op jit(solution)/shard_map/pallas_call | solution.py:399
  77.0 0.7 shard_map.186

commit v5 on v4

--- a/solution.py
+++ b/solution.py
@@ -13,11 +13,11 @@
 PLACES = 8 * Z
 EPS = 1e-06
 W1 = 640
-FFY = 352
-FP = 384
-W2 = 2 * FP
-PH = 16
-S_Z, S_M, S_C, S_H, S_G, S_A, S_F, S_O, S_WO, S_WG, S_WD, S_GN, S_Y = range(PH - 3)
+FFZ = 176
+FHALF = 192
+FP = 2 * FHALF
+PH = 17
+S_Z, S_M, S_C, S_H, S_G, S_A, S_F, S_O, S_WO, S_WG, S_WD, S_GN, S_WZ, S_Y = range(PH - 3)
 PARTS = 4
 SLOTS = Z // PARTS
 
@@ -42,7 +42,7 @@
     refs = refs[IN_NAMES + 2 :]
     own, refs = refs[:IN_NAMES], refs[IN_NAMES:]
     (
-        part, yrecv, zs1, zr1, mrecv, cs, cr, hbuf, wgs, wgr, wob, wds, wdb, gl, gb, zs2, zr2, ab, fs, fr, ob, hct, wab,
+        part, yrecv, zs1, zr1, mrecv, cs, cr, hbuf, wgs, wst, wgr, wob, wds, wdb, gl, gb, zs2, zr2, ab, fs, fr, ob, hct, wab,
         send, recv, load, known,
     ) = refs
     (
@@ -54,6 +54,8 @@
     z = kv // Y
     y = kv % Y
     group = y * TP + tp
+    bit = z % 2
+    twin = z + 1 - 2 * bit
 
     def y_peer(k):
         return z * Y + (y + k) % Y
@@ -132,12 +134,14 @@
         if k not in first:
             loads[k].wait()
     for k in range(Y):
-        wgs[k, :, 0:FFY] = wgate_ref[:, FFY * k : FFY * (k + 1)]
-        wgs[k, :, FFY:FP] = jnp.zeros((64, FP - FFY), BF16)
-        wgs[k, :, FP : FP + FFY] = wup_ref[:, FFY * k : FFY * (k + 1)]
-        wgs[k, :, FP + FFY : W2] = jnp.zeros((64, FP - FFY), BF16)
-        wds[k, :, 0:FFY] = wdown_ref[:, FFY * k : FFY * (k + 1)]
-        wds[k, :, FFY:FP] = jnp.zeros((64, FP - FFY), BF16)
+        for n in range(2):
+            cut, low = slice(FFZ * (2 * k + n), FFZ * (2 * k + n + 1)), FHALF * n
+            wgs[n, k, :, 0:FFZ] = wgate_ref[:, cut]
+            wgs[n, k, :, FFZ:FHALF] = jnp.zeros((64, FHALF - FFZ), BF16)
+            wgs[n, k, :, FHALF : FHALF + FFZ] = wup_ref[:, cut]
+            wgs[n, k, :, FHALF + FFZ : FP] = jnp.zeros((64, FHALF - FFZ), BF16)
+            wds[k, :, low : low + FFZ] = wdown_ref[:, cut]
+            wds[k, :, low + FFZ : low + FHALF] = jnp.zeros((64, FHALF - FFZ), BF16)
     gl[...] = jnp.zeros((8, 128), F32) + jnp.concatenate([mgain_ref[...], mgain_ref[...]], axis=1)
 
     pl.semaphore_wait(barrier, 8 + Y * TP - 1)
@@ -149,18 +153,18 @@
         for k in range(1, Y):
             peer = y_peer(k)
             rcopy(part.at[peer % Y, some], yrecv.at[y, some], S_Y + c, (peer, tp)).start()
+    rcopy(wgs.at[1 - bit], wst.at[bit], S_WZ, (twin * Y + y, tp)).start()
     for k in range(1, Y):
         peer = y_peer(k)
         rcopy(wout_ref, wob.at[y], S_WO, (peer, tp)).start()
-        rcopy(wgs.at[peer % Y], wgr.at[y], S_WG, (peer, tp)).start()
         rcopy(wds.at[peer % Y], wdb.at[y], S_WD, (peer, tp)).start()
-        rcopy(gl, gb.at[y], S_GN, (peer, tp)).start()
+        rcopy(gl, gb.at[bit * Y + y], S_GN, (peer, tp)).start()
 
     yrecv[y] = part[y]
     wob[y] = wout_ref[...]
-    wgr[y] = wgs[y]
+    wst[bit] = wgs[bit]
     wdb[y] = wds[y]
-    gb[y] = gl[...]
+    gb[bit * Y + y] = gl[...]
 
     def send_z1(j, c):
         to = z_peer(j)
@@ -177,6 +181,14 @@
         zs1[low:high_slot] = total.astype(BF16)
         lax.fori_loop(low, min(high_slot, Z - 1), send_z1, 0, unroll=True)
     zr1[z] = zs1[Z - 1]
+    arrived(wst.at[0], S_WZ)
+    for k in range(Y):
+        rcopy(gl, gb.at[bit * Y + y], S_GN, (twin * Y + (y + k) % Y, tp)).start()
+    for k in range(1, Y):
+        peer = y_peer(k)
+        for n in range(2):
+            rcopy(wst.at[n, peer % Y], wgr.at[n, y], S_WG, (peer, tp)).start()
+    wgr[:, y] = wst[:, y]
 
     seq = iota((SEQS, ROWS), 0)
     lens8 = jnp.concatenate([lens_ref[...], lens_ref[...]], axis=1).astype(F32) + jnp.zeros((8, 128), F32)
@@ -246,11 +258,13 @@
     lax.fori_loop(0, Z - 1, send_m, 0, unroll=True)
     arrived(wob.at[0:3], S_WO)
     wo = wob[...].reshape(256, 256)
-    arrived(gb.at[0:3], S_GN)
+    arrived(gb.at[0 : 2 * Y - 1], S_GN)
     low_lane = iota((1, 128), 1) < 64
-    gain = jnp.concatenate(
-        [jnp.where(low_lane, gb[0, 0:1], gb[1, 0:1]), jnp.where(low_lane, gb[2, 0:1], gb[3, 0:1])], axis=1
-    )
+
+    def gain_of(n):
+        row = [gb[n * Y + k, 0:1] for k in range(Y)]
+        return jnp.concatenate([jnp.where(low_lane, row[0], row[1]), jnp.where(low_lane, row[2], row[3])], axis=1)
+
     low_half = iota((8, 128), 0) < 4
 
     def slot_of(where):
@@ -288,23 +302,30 @@
             rcopy(cs.at[where[1]], cr.at[tp], S_C, where).start()
     cr[tp] = cs[tp]
     arrived(cr.at[0 : TP - 1], S_C)
-    hbuf[group] = (residual + jnp.sum(cr[...].astype(F32), axis=0)).astype(BF16)
-
+    place_h = bit * Y * TP + group
+    hbuf[place_h] = (residual + jnp.sum(cr[...].astype(F32), axis=0)).astype(BF16)
+    for d in apart + [(0, 0, 0)]:
+        other, where = group_peer(d)
+        rcopy(hbuf.at[place_h], hbuf.at[place_h], S_H, (where[0] + (twin - z) * Y, where[1])).start()
     for d in apart:
         other, where = group_peer(d)
-        rcopy(hbuf.at[group], hbuf.at[group], S_H, where).start()
-    arrived(wgr.at[0:3], S_WG)
-    arrived(hbuf.at[0 : Y * TP - 1], S_H)
-
-    hidden = mm(pick, hbuf[...].astype(F32).reshape(ROWS, 256).astype(BF16))
-    hscaled = (hidden * gain).astype(BF16)
-    products = mm(hscaled, wgr[...].reshape(256, W2))
+        rcopy(hbuf.at[place_h], hbuf.at[place_h], S_H, where).start()
+    arrived(wgr.at[:, 0:3], S_WG)
+    gains = gain_of(bit), gain_of(1 - bit)
+    arrived(hbuf.at[0 : 2 * Y * TP - 1], S_H)
+
+    def chosen(n):
+        return mm(pick, hbuf[pl.ds(n * Y * TP, Y * TP)].astype(F32).reshape(ROWS, 256).astype(BF16))
+
+    hidden, beside = chosen(bit), chosen(1 - bit)
+    products = mm((hidden * gains[0]).astype(BF16), wgr[bit].reshape(256, FP))
+    products = products + mm((beside * gains[1]).astype(BF16), wgr[1 - bit].reshape(256, FP))
     squares2 = jnp.sum(hidden * hidden, axis=1, keepdims=True)
     high2 = squares2.astype(BF16).astype(F32)
     low2 = squares2 - high2
-    lane2 = iota((PLACES, W2), 1)
-    products = jnp.where(lane2 == FFY, high2, jnp.where(lane2 == FFY + 1, low2, products))
-    zs2[...] = products.reshape(Z, 8, W2).astype(BF16)
+    lane2 = iota((PLACES, FP), 1)
+    products = jnp.where(lane2 == FFZ, high2, jnp.where(lane2 == FFZ + 1, low2, products))
+    zs2[...] = products.reshape(Z, 8, FP).astype(BF16)
 
     def send_g(j, c):
         to = z_peer(j)
@@ -316,13 +337,18 @@
     hct[...] = hidden.T
     arrived(wdb.at[0:3], S_WD)
     arrived(zr2.at[0 : Z - 1], S_G)
-    summed = jnp.sum(zr2[...].astype(F32), axis=0)
+    summed = jnp.sum(zr2[...].astype(F32).reshape(Z // 2, 2, 8, FP), axis=0)
     lane3 = iota((8, FP), 1)
-    gate, up = summed[:, 0:FP], summed[:, FP:W2]
-    total2 = jnp.sum(jnp.where((lane3 == FFY) | (lane3 == FFY + 1), gate, 0.0), axis=1, keepdims=True)
+    both = summed[0] + summed[1]
+    total2 = jnp.sum(jnp.where((lane3 == FFZ) | (lane3 == FFZ + 1), both, 0.0), axis=1, keepdims=True)
     rstd2 = lax.rsqrt(total2 / D + EPS)
-    gate = jnp.where(lane3 < FFY, gate, 0.0) * rstd2
-    ab[z] = (gate * jax.nn.sigmoid(gate) * (up * rstd2)).astype(BF16)
+
+    def activated(n):
+        gate = jnp.where(lane3 < FFZ, summed[n], 0.0) * rstd2
+        up = pltpu.roll(summed[n], FHALF, 1) * rstd2
+        return gate * jax.nn.sigmoid(gate) * up
+
+    ab[z] = (activated(0) + pltpu.roll(activated(1), FHALF, 1)).astype(BF16)
 
     def send_a(j, c):
         rcopy(ab.at[z], ab.at[z], S_A, (z_peer(j) * Y + y, tp)).start()
@@ -332,29 +358,29 @@
     arrived(ab.at[0 : Z - 1], S_A)
 
     active = ab[...].astype(F32).reshape(PLACES, FP).astype(BF16)
-    fs[...] = mmt(wdb[...].reshape(256, FP), active).reshape(Y * TP, 8, 128).astype(BF16)
-
+    fs[...] = mmt(wdb[...].reshape(256, FP), active).reshape(2 * Y, 32, 128).astype(BF16)
+    x, core = tp // 2, tp % 2
     for d in apart:
-        other, where = group_peer(d)
-        rcopy(fs.at[other], fr.at[group], S_F, where).start()
-    fr[group] = fs[group]
-    arrived(fr.at[0 : Y * TP - 1], S_F)
-    ended = jnp.sum(fr[...].astype(F32), axis=0) + hct[pl.ds(pl.multiple_of(8 * group, 8), 8), :]
-    ob[tp] = ended.astype(BF16)
-
+        if d[1] == 0:
+            to_y, to_core = (y + d[0]) % Y, (core + d[2]) % 2
+            rcopy(fs.at[to_y * 2 + to_core], fr.at[y * 2 + core], S_F, (z * Y + to_y, x * 2 + to_core)).start()
+    fr[y * 2 + core] = fs[y * 2 + core]
+    arrived(fr.at[0 : 2 * Y - 1], S_F)
+    ob[tp] = jnp.sum(fr[...].astype(F32), axis=0).astype(BF16)
     for d in apart:
         if d[0] == 0:
             other, where = group_peer(d)
             rcopy(ob.at[tp], ob.at[tp], S_O, where).start()
     arrived(ob.at[0 : TP - 1], S_O)
-    final = ob[...].astype(F32).reshape(64, PLACES).astype(BF16)
+    fed = jnp.sum(ob[...].astype(F32).reshape(X, 64, 128), axis=0)
+    final = (fed + hct[pl.ds(pl.multiple_of(64 * y, 64), 64), :]).astype(BF16)
     out_ref[...] = mm(final, give).astype(BF16)
 
     for ref, phase in (
         (zr1.at[0 : Z - 1], S_Z), (mrecv.at[0 : Z - 1], S_M), (cr.at[0 : TP - 1], S_C),
-        (hbuf.at[0 : Y * TP - 1], S_H), (zr2.at[0 : Z - 1], S_G), (ab.at[0 : Z - 1], S_A),
-        (fr.at[0 : Y * TP - 1], S_F), (ob.at[0 : TP - 1], S_O), (wob.at[0:3], S_WO), (wgr.at[0:3], S_WG),
-        (wdb.at[0:3], S_WD), (gb.at[0:3], S_GN),
+        (hbuf.at[0 : 2 * Y * TP - 1], S_H), (zr2.at[0 : Z - 1], S_G), (ab.at[0 : Z - 1], S_A),
+        (fr.at[0 : 2 * Y - 1], S_F), (ob.at[0 : TP - 1], S_O), (wob.at[0:3], S_WO), (wgr.at[:, 0:3], S_WG), (wst.at[0], S_WZ),
+        (wdb.at[0:3], S_WD), (gb.at[0 : 2 * Y - 1], S_GN),
     ):
         sent(ref, phase)
     for c in range(PARTS):
@@ -379,20 +405,21 @@
         ((Z, 8, 128), BF16),
         ((TP, 8, 256), BF16),
         ((TP, 8, 256), BF16),
-        ((Y * TP, 8, 256), BF16),
-        ((Y, 64, W2), BF16),
-        ((Y, 64, W2), BF16),
+        ((2 * Y * TP, 8, 256), BF16),
+        ((2, Y, 64, FP), BF16),
+        ((2, Y, 64, FP), BF16),
+        ((2, Y, 64, FP), BF16),
         ((Y, 64, 256), BF16),
         ((Y, 64, FP), BF16),
         ((Y, 64, FP), BF16),
         ((8, 128), F32),
-        ((Y, 8, 128), F32),
-        ((Z, 8, W2), BF16),
-        ((Z, 8, W2), BF16),
+        ((2 * Y, 8, 128), F32),
         ((Z, 8, FP), BF16),
-        ((Y * TP, 8, 128), BF16),
-        ((Y * TP, 8, 128), BF16),
-        ((TP, 8, 128), BF16),
+        ((Z, 8, FP), BF16),
+        ((Z, 8, FP), BF16),
+        ((2 * Y, 32, 128), BF16),
+        ((2 * Y, 32, 128), BF16),
+        ((TP, 32, 128), BF16),
         ((256, 128), F32),
         ((128, 64), BF16),
     ]

time: 77.9 us -> 73.7 us (0.946)
  Pallas kernels: 77.1 us -> 72.9 us
    pallas_call x1, Pallas kernels: 76.4 us -> 72.2 us  [per_device(): pl.pallas_call(kernel, out_shape=tuple((pltpu.VMEM(a.shape, a.dtype) for...]
where the time goes in v5:
time: 73.7 us; the launch traced here: 73.5 us
  Pallas kernels  72.9 us (99%)
    pallas_call x1, Pallas kernels, per_device(): pl.pallas_call(kernel, out_shape=tuple((pltpu.VMEM(a.shape, a.dtype) for...  72.2 us

profile of v5, /device:TPU:1, one launch (start us, length us, event | category | flops | bytes accessed | tf_op | source)
XLA Modules:
  0.0 73.5 jit_solution(11604595195853439048)
XLA Ops:
  0.6 72.2 %shard_map.185 = (bf16[64,256]{1,0:T(8,128)(2,1)S(1)}, f32[1,2,128,128]{3,2,1,0:T(8,128)S(1)}) custom-call(bf16[64,256]{1,0:T(8,128)(2,1)} %bitcast.13, s32[1,64]{1,0:T(1,128)} %bitcast.17, f32[1,2,128,128]{3,2,1,0:T(8,128)} %refs_2_.1, f32[1,64]{1,0:T(1,128)} %bitcast.18, bf16[64,256]{1,0:T(8,128)(2,1)} %refs_4_.1, bf16[64,256]{1,0:T(8,128)(2,1)} %refs_5_.1, ...), custom_call_target="tpu_custom_call" | custom-call | tf_op jit(solution)/shard_map/pallas_call | solution.py:426
  72.8 0.7 shard_map.186

commit v6 on v5

--- a/solution.py
+++ b/solution.py
@@ -12,13 +12,13 @@
 ROWS = SEQS * NEW
 PLACES = 8 * Z
 EPS = 1e-06
-W1 = 640
+W1 = 512
 FFZ = 176
 FHALF = 192
 FP = 2 * FHALF
-PH = 17
-S_Z, S_M, S_C, S_H, S_G, S_A, S_F, S_O, S_WO, S_WG, S_WD, S_GN, S_WZ, S_Y = range(PH - 3)
-PARTS = 4
+S_Z, S_M, S_C, S_H, S_G, S_A, S_F, S_O, S_WO, S_WG, S_WD, S_GN, S_WZ, S_TK, S_EY, S_EZ, S_Y = range(17)
+PARTS = 8
+PH = 17 + PARTS
 SLOTS = Z // PARTS
 
 
@@ -42,7 +42,7 @@
     refs = refs[IN_NAMES + 2 :]
     own, refs = refs[:IN_NAMES], refs[IN_NAMES:]
     (
-        part, yrecv, zs1, zr1, mrecv, cs, cr, hbuf, wgs, wst, wgr, wob, wds, wdb, gl, gb, zs2, zr2, ab, fs, fr, ob, hct, wab,
+        part, yrecv, zs1, zr1, eys, eyr, ezs, ezr, tks, tkr, mrecv, cs, cr, hbuf, wgs, wst, wgr, wob, wds, wdb, gl, gb, zs2, zr2, ab, fs, fr, ob, hct,
         send, recv, load, known,
     ) = refs
     (
@@ -113,22 +113,23 @@
     turn = jnp.where(row == wanted, 1.0, 0.0).astype(BF16)
     xt = mmt(turn, tok_ref[...])
     xs = (xt * ngain_ref[...]).astype(BF16)
-    wab[...] = jnp.zeros((128, 64), BF16)
-    wab[64:80, :] = wa_ref[...]
-    wab[80:96, :] = wb_ref[...]
+    kind, source = iota((128, 32), 0) & 7, iota((128, 32), 1)
+    both_w = jnp.concatenate([wa_ref[...], wb_ref[...]], axis=0)
+    from_where = jnp.where(kind < 2, 2 * tp + kind, 14 + 2 * tp + kind)
+    chosen_w = jnp.where((source == from_where) & (kind < 4), 1.0, 0.0).astype(BF16)
+    wab = mm(chosen_w, both_w).astype(BF16)
     squares = jnp.sum(xt * xt, axis=1, keepdims=True)
-    high = squares.astype(BF16).astype(F32)
-    low = squares - high
     eye = jnp.where(iota((64, 128), 0) == iota((64, 128), 1), 1.0, 0.0).astype(BF16)
     lane = iota((2 * ROWS, 128), 1)
-    extra = mmt(xs, wab[...]) + mm(xt.astype(BF16), eye)
-    extra = jnp.where(lane == 96, high, jnp.where(lane == 97, low, extra))
+    extra = jnp.where((lane & 7) == 4, squares, mmt(xs, wab))
+    extra = jnp.where((lane >> 3) == (iota((2 * ROWS, 128), 0) & 7), extra, 0.0)
+    eys[...] = jnp.sum(extra.reshape(Y, Z, 8, 128), axis=2)
+    tks[...] = mm(xt.astype(BF16), eye).reshape(Y, Z, 8, 128).astype(BF16)
     second = (iota((2 * ROWS, 256), 0) & 4) == 4
     left = jnp.where(second, mm(xs, wv_ref[...]), mm(xs, wq_ref[...]))
     part[:, :, :, 0:256] = left.reshape(Y, Z, 8, 256).astype(BF16)
     right = jnp.where(second, mm(xs, wg_ref[...]), mm(xs, wk_ref[...]))
     part[:, :, :, 256:512] = right.reshape(Y, Z, 8, 256).astype(BF16)
-    part[:, :, :, 512:640] = extra.reshape(Y, Z, 8, 128).astype(BF16)
 
     for k in range(IN_NAMES):
         if k not in first:
@@ -148,6 +149,9 @@
 
     for k in (4, -4):
         pl.semaphore_signal(known, inc=1, device_id=z_near(k), device_id_type=MESH)
+    for k in range(1, Y):
+        peer = y_peer(k)
+        rcopy(eys.at[peer % Y], eyr.at[y], S_EY, (peer, tp)).start()
     for c in range(PARTS):
         some = pl.ds(SLOTS * c, SLOTS)
         for k in range(1, Y):
@@ -157,10 +161,13 @@
     for k in range(1, Y):
         peer = y_peer(k)
         rcopy(wout_ref, wob.at[y], S_WO, (peer, tp)).start()
+        rcopy(tks.at[peer % Y], tkr.at[y], S_TK, (peer, tp)).start()
         rcopy(wds.at[peer % Y], wdb.at[y], S_WD, (peer, tp)).start()
         rcopy(gl, gb.at[bit * Y + y], S_GN, (peer, tp)).start()
 
     yrecv[y] = part[y]
+    eyr[y] = eys[y]
+    tkr[y] = tks[y]
     wob[y] = wout_ref[...]
     wst[bit] = wgs[bit]
     wdb[y] = wds[y]
@@ -171,7 +178,19 @@
         rcopy(zs1.at[j], zr1.at[z], S_Z, (to * Y + y, tp)).start()
         return c
 
+    def send_e(j, c):
+        to = z_peer(j)
+        rcopy(ezs.at[j], ezr.at[z], S_EZ, (to * Y + y, tp)).start()
+        return c
+
+    arrived(eyr.at[0:3], S_EY)
+    lines = eyr[0]
+    for k in range(1, Y):
+        lines = lines + eyr[k]
+    ezs[...] = lines.reshape(Z, 1, 128)
+    ezr[z] = ezs[Z - 1]
     pl.semaphore_wait(known, 2)
+    lax.fori_loop(0, Z - 1, send_e, 0, unroll=True)
     for c in range(PARTS):
         low, high_slot = SLOTS * c, SLOTS * (c + 1)
         arrived(yrecv.at[0:3, low:high_slot], S_Y + c)
@@ -211,21 +230,22 @@
     arrived(zr1.at[0 : Z - 1], S_Z)
 
     mine = jnp.sum(zr1[...].astype(F32), axis=0)
+    arrived(ezr.at[0 : Z - 1], S_EZ)
+    ext = jnp.sum(ezr[...], axis=0)
     lane8 = iota((8, 128), 1)
-    ext = mine[:, 512:640]
+    slot8 = 8 * (iota((8, 128), 0) & 3)
 
     def lane_of(values, where):
-        return jnp.sum(jnp.where(lane8 == where, values, 0.0), axis=1, keepdims=True)
-
-    rstd = lax.rsqrt((lane_of(ext, 96) + lane_of(ext, 97)) / D + EPS)
-    main = (mine[:, 0:512] * rstd).astype(BF16).astype(F32)
-    ext = ext * rstd
+        return jnp.sum(jnp.where(lane8 == slot8 + where, values, 0.0), axis=1, keepdims=True)
+
+    rstd = lax.rsqrt(lane_of(ext, 4) / D + EPS)
+    main = (mine * rstd).astype(BF16).astype(F32)
     length = jnp.sum(jnp.where(iota((1, SEQS), 1) == kv, lens_ref[...], 0), axis=1, keepdims=True)
     live = iota((8, 1), 0) < length
     rows = []
     for h in range(2):
-        alpha = lane_of(ext, 64 + 2 * tp + h)
-        beta = jax.nn.sigmoid(lane_of(ext, 80 + 2 * tp + h))
+        alpha = lane_of(ext, h) * rstd
+        beta = jax.nn.sigmoid(lane_of(ext, 2 + h) * rstd)
         shifted = alpha + dbias_ref[:, h : h + 1]
         soft = jnp.maximum(shifted, 0.0) + jnp.log1p(jnp.exp(-jnp.abs(shifted)))
         rate = jnp.exp(jnp.zeros((8, 1), F32) + dlog_ref[:, h : h + 1])
@@ -271,11 +291,13 @@
         away = (where - z + Z) % Z
         return (1 - away // 8) * (15 - 2 * away) + (away // 8) * (2 * away - 16)
 
+    arrived(tkr.at[0:3], S_TK)
+
     def kept(k):
         return jnp.where(
             low_half,
-            yrecv[k, slot_of(2 * tp), :, 512:640].astype(F32),
-            yrecv[k, slot_of(2 * tp + 1), :, 512:640].astype(F32),
+            tkr[k, slot_of(2 * tp)].astype(F32),
+            tkr[k, slot_of(2 * tp + 1)].astype(F32),
         )
 
     residual = jnp.concatenate(
@@ -377,7 +399,7 @@
     out_ref[...] = mm(final, give).astype(BF16)
 
     for ref, phase in (
-        (zr1.at[0 : Z - 1], S_Z), (mrecv.at[0 : Z - 1], S_M), (cr.at[0 : TP - 1], S_C),
+        (zr1.at[0 : Z - 1], S_Z), (tkr.at[0:3], S_TK), (eyr.at[0:3], S_EY), (ezr.at[0 : Z - 1], S_EZ), (mrecv.at[0 : Z - 1], S_M), (cr.at[0 : TP - 1], S_C),
         (hbuf.at[0 : 2 * Y * TP - 1], S_H), (zr2.at[0 : Z - 1], S_G), (ab.at[0 : Z - 1], S_A),
         (fr.at[0 : 2 * Y - 1], S_F), (ob.at[0 : TP - 1], S_O), (wob.at[0:3], S_WO), (wgr.at[:, 0:3], S_WG), (wst.at[0], S_WZ),
         (wdb.at[0:3], S_WD), (gb.at[0 : 2 * Y - 1], S_GN),
@@ -402,6 +424,12 @@
     )
     outputs = (jax.ShapeDtypeStruct((64, ROWS), BF16), jax.ShapeDtypeStruct(memory.shape, F32))
     shapes = [((Y, Z, 8, W1), BF16)] * 2 + [((Z, 8, W1), BF16)] * 2 + [
+        ((Y, Z, 128), F32),
+        ((Y, Z, 128), F32),
+        ((Z, 1, 128), F32),
+        ((Z, 1, 128), F32),
+        ((Y, Z, 8, 128), BF16),
+        ((Y, Z, 8, 128), BF16),
         ((Z, 8, 128), BF16),
         ((TP, 8, 256), BF16),
         ((TP, 8, 256), BF16),
@@ -421,7 +449,6 @@
         ((2 * Y, 32, 128), BF16),
         ((TP, 32, 128), BF16),
         ((256, 128), F32),
-        ((128, 64), BF16),
     ]
     result, new_memory = pl.pallas_call(
         kernel,

time: 73.7 us -> 73.2 us (level)
  no operation moved by 1% of the time
where the time goes in v6:
time: 73.2 us; the launch traced here: 73 us
  Pallas kernels  72.4 us (99%)
    pallas_call x1, Pallas kernels, per_device(): pl.pallas_call(kernel, out_shape=tuple((pltpu.VMEM(a.shape, a.dtype) for...  71.7 us

profile of v6, /device:TPU:1, one launch (start us, length us, event | category | flops | bytes accessed | tf_op | source)
XLA Modules:
  0.0 73.0 jit_solution(11835648483656576457)
XLA Ops:
  0.6 71.7 %shard_map.185 = (bf16[64,256]{1,0:T(8,128)(2,1)S(1)}, f32[1,2,128,128]{3,2,1,0:T(8,128)S(1)}) custom-call(bf16[64,256]{1,0:T(8,128)(2,1)} %bitcast.13, s32[1,64]{1,0:T(1,128)} %bitcast.17, f32[1,2,128,128]{3,2,1,0:T(8,128)} %refs_2_.1, f32[1,64]{1,0:T(1,128)} %bitcast.18, bf16[64,256]{1,0:T(8,128)(2,1)} %refs_4_.1, bf16[64,256]{1,0:T(8,128)(2,1)} %refs_5_.1, ...), custom_call_target="tpu_custom_call" | custom-call | tf_op jit(solution)/shard_map/pallas_call | solution.py:453
  72.3 0.7 shard_map.186
